TPU v7x, 128 devices: a whole 4x4x4 slice. The times are simulated.
128 devices in a mesh: kv: 16 (over z, x), tp: 8 (over y, core).
Axes of the slice: x: 4, y: 4, z: 4, core: 2. Of those that a mesh axis runs over, the one named last changes fastest.
Arguments:
- hidden: bfloat16 [1024, 4096], P(None, 'kv'), as said below
- norm_gain: bfloat16 [4096], replicated, may hold values from 0.099609375 to 1.8984375
- w_query: bfloat16 [4096, 4096], P('kv', 'tp'), may hold values from -0.09375 to 0.09375
- w_key: bfloat16 [4096, 4096], P('kv', 'tp'), may hold values from -0.09375 to 0.09375
- w_value: bfloat16 [4096, 8192], P('kv', 'tp'), may hold values from -0.09375 to 0.09375
- w_gate: bfloat16 [4096, 8192], P('kv', 'tp'), may hold values from -0.09375 to 0.09375
- w_write: bfloat16 [4096, 32], P('kv', 'tp'), may hold values from -0.09375 to 0.09375
- w_decay: bfloat16 [4096, 32], P('kv', 'tp'), may hold values from -0.09375 to 0.09375
- w_out: bfloat16 [8192, 4096], P('tp', 'kv'), may hold values from -0.0625 to 0.0625
- decay_rate: float32 [32], P('tp'), may hold values from 0 to 4, as said below
- head_gain: float32 [256], replicated, may hold values from 0.1 to 1.9
- carried_state: float32 [256, 32, 128, 256], P('kv', 'tp'), may hold values from -4 to 4
- last_keys: bfloat16 [256, 4, 4096], P('kv', None, 'tp'), may hold values from -6 to 6
- last_values: bfloat16 [256, 4, 8192], P('kv', None, 'tp'), may hold values from -6 to 6
- last_writes: float32 [256, 4, 32], P('kv', None, 'tp'), may hold values from -6 to 6
- last_decays: float32 [256, 4, 32], P('kv', None, 'tp'), may hold values from -6 to 6
- accepted: int32 [256], P('kv'), may hold values from 0 to 4
Outputs:
- mixed_out: bfloat16 [1024, 4096], P('tp', 'kv')
- committed: float32 [256, 32, 128, 256], P('kv', 'tp')
Inputs may be any that keep to these rules, and one draw needn't show every extreme that they name: `decay_rate`: positive. `hidden`: finite real values.
All inputs are finite; a program needn't handle non-finite values.
Results may differ from a plain program's by a relative error of at most 0.029.
Values may be sent and summed in bfloat16 or wider, within the bound.
A program may use at most 128 MiB of HBM per device.

v0:
```python
import jax
import jax.numpy as jnp
from jax import lax
from jax.sharding import PartitionSpec as P

D = 4096


norm_eps = 1e-06


def in_one_piece(arrays, axis, dim, along):
    columns = [a.reshape(*a.shape[:along], -1) for a in arrays]
    both = jnp.concatenate(columns, axis=along)
    out, at, finished = (lax.psum_scatter(both, axis, scatter_dimension=dim, tiled=True), 0, [])
    for a, column in zip(arrays, columns):
        section = out[..., at : at + column.shape[along]]
        finished.append(section.reshape(*section.shape[:along], *a.shape[along:]))
        at += column.shape[along]
    return tuple(finished)


def sent_to_all(value, axis):
    copies = jnp.broadcast_to(value, (lax.axis_size(axis), *value.shape))
    return lax.all_to_all(copies, axis, split_axis=0, concat_axis=0, tiled=True)


def laid_out(blocks, dim):
    blocks = jnp.moveaxis(blocks, 0, dim)
    dims = blocks.shape
    return blocks.reshape(*dims[:dim], dims[dim] * dims[dim + 1], *dims[dim + 2 :])


def collect(value, axis, dim):
    blocks = sent_to_all(value, axis)
    return laid_out(blocks, dim)


def in_blocks(value, dim, count):
    dims = value.shape
    blocks = value.reshape(*dims[:dim], count, dims[dim] // count, *dims[dim + 1 :])
    return jnp.moveaxis(blocks, dim, 0)


def sent_and_summed(value, axis, dim):
    count = lax.axis_size(axis)
    blocks = lax.all_to_all(in_blocks(value, dim, count), axis, 0, 0, tiled=True)
    return jnp.sum(blocks.astype(jnp.float32), axis=0)


def unit_rows(matrix):
    return matrix * lax.rsqrt(jnp.sum(matrix * matrix, -1, keepdims=True) + norm_eps)


def corrected(key_rows, values, write_rate, log_decay, start_state):
    proposals = key_rows.shape[2]
    value_width = values.shape[-1]
    running = jnp.cumsum(log_decay, axis=-1)
    causal = jnp.tril(jnp.ones((proposals, proposals), dtype=bool))
    spread = running[..., :, None] - running[..., None, :]
    weights = jnp.where(causal, jnp.exp(jnp.where(causal, spread, 0.0)), 0.0)
    strong_keys = key_rows * write_rate[..., None]
    lower_part = jnp.einsum("bhcd,bhsd->bhcs", strong_keys, key_rows)
    lower_part = lower_part * weights * (1.0 - jnp.eye(proposals, dtype=jnp.float32))
    right_side = jnp.concatenate(
        [values * write_rate[..., None], strong_keys * jnp.exp(running)[..., None]], -1
    )
    solved_rows = []
    for later in range(proposals):
        current = right_side[..., later, :]
        for early in range(later):
            current = current - lower_part[..., later, early, None] * solved_rows[early]
        solved_rows.append(current)
    solved = jnp.stack(solved_rows, axis=2)
    fresh_values = solved[..., :value_width] - jnp.einsum(
        "bhcd,bhde->bhce", solved[..., value_width:], start_state
    )
    return (fresh_values, running, weights)


def advance(key_rows, fresh_values, running, start_state):
    tail_decay = jnp.exp(running[..., -1:] - running)
    return start_state * jnp.exp(running[..., -1])[..., None, None] + jnp.einsum(
        "bhcd,bhce->bhde", key_rows * tail_decay[..., None], fresh_values
    )


def readout(queries, key_rows, fresh_values, running, weights, start_state):
    scores = jnp.einsum("bhcd,bhsd->bhcs", queries, key_rows) * weights
    carried = jnp.einsum("bhcd,bhde->bhce", queries * jnp.exp(running)[..., None], start_state)
    return carried + jnp.einsum("bhcs,bhse->bhce", scores, fresh_values)


def core(
    proj_query,
    proj_key,
    proj_value,
    proj_gate,
    proj_write,
    proj_decay,
    decay_rate,
    head_gain,
    carried_state,
    last_keys,
    last_values,
    last_writes,
    last_decays,
    accepted,
):
    seq_count, head_count, key_width, value_width = carried_state.shape
    proposals = last_keys.shape[1]

    def by_head(matrix, width):
        return jnp.transpose(matrix.reshape(seq_count, proposals, head_count, width), (0, 2, 1, 3))

    def by_head_small(matrix):
        return jnp.transpose(matrix.reshape(seq_count, proposals, head_count), (0, 2, 1))

    rates = decay_rate[None, :, None]
    taken = (jnp.arange(proposals, dtype=jnp.int32)[None, :] < accepted[:, None]).astype(
        jnp.float32
    )[:, None, :]
    old_keys = unit_rows(by_head(last_keys.astype(jnp.float32), key_width))
    old_values = by_head(last_values.astype(jnp.float32), value_width)
    old_write = jax.nn.sigmoid(by_head_small(last_writes)) * taken
    old_decay = -rates * jax.nn.softplus(by_head_small(last_decays)) * taken
    fresh_values, running, weights = corrected(
        old_keys, old_values, old_write, old_decay, carried_state
    )
    committed = advance(old_keys, fresh_values, running, carried_state)
    queries = unit_rows(by_head(jax.nn.silu(proj_query), key_width)) * key_width ** (-0.5)
    key_rows = unit_rows(by_head(jax.nn.silu(proj_key), key_width))
    values = by_head(jax.nn.silu(proj_value), value_width)
    write_rate = jax.nn.sigmoid(by_head_small(proj_write))
    log_decay = -rates * jax.nn.softplus(by_head_small(proj_decay))
    fresh_values, running, weights = corrected(key_rows, values, write_rate, log_decay, committed)
    result = readout(queries, key_rows, fresh_values, running, weights, committed)
    normed = result * lax.rsqrt(jnp.mean(result * result, -1, keepdims=True) + norm_eps) * head_gain
    gated = normed * jax.nn.silu(by_head(proj_gate, value_width))
    gated_rows = (
        jnp.transpose(gated, (0, 2, 1, 3))
        .reshape(seq_count * proposals, head_count * value_width)
        .astype(jnp.bfloat16)
    )
    return (gated_rows, committed)


def per_device(
    hidden,
    norm_gain,
    w_query,
    w_key,
    w_value,
    w_gate,
    w_write,
    w_decay,
    w_out,
    decay_rate,
    head_gain,
    carried_state,
    last_keys,
    last_values,
    last_writes,
    last_decays,
    accepted,
):
    local_width = hidden.shape[1]
    weight_set = (w_query, w_key, w_value, w_gate, w_write, w_decay)
    wide_rows = hidden.astype(jnp.float32)
    local_sq = jnp.sum(wide_rows * wide_rows, -1)
    gain_part = lax.dynamic_slice_in_dim(norm_gain, lax.axis_index("kv") * local_width, local_width)
    scaled = (wide_rows * gain_part.astype(jnp.float32)).astype(jnp.bfloat16)
    terms = tuple(
        (jnp.dot(scaled, weight, preferred_element_type=jnp.float32) for weight in weight_set)
    )
    summed = tuple(
        (
            part.astype(jnp.float32)
            for part in in_one_piece(
                (
                    terms[0].astype(jnp.bfloat16),
                    terms[1].astype(jnp.bfloat16),
                    terms[2].astype(jnp.bfloat16),
                    terms[3].astype(jnp.bfloat16),
                    terms[4].astype(jnp.bfloat16),
                    terms[5].astype(jnp.bfloat16),
                    local_sq.astype(jnp.bfloat16),
                ),
                "kv",
                0,
                1,
            )
        )
    )
    projected = summed[:6]
    own_sq = summed[6]
    inverse = lax.rsqrt(own_sq / D + norm_eps)[:, None]
    normal_proj = tuple((matrix * inverse for matrix in projected))
    gated_rows, committed = core(
        normal_proj[0],
        normal_proj[1],
        normal_proj[2],
        normal_proj[3],
        normal_proj[4],
        normal_proj[5],
        decay_rate,
        head_gain,
        carried_state,
        last_keys,
        last_values,
        last_writes,
        last_decays,
        accepted,
    )
    partial_out = jnp.dot(collect(gated_rows, "kv", 0), w_out, preferred_element_type=jnp.float32)
    mixed_out = sent_and_summed(partial_out.astype(jnp.bfloat16), "tp", 0).astype(jnp.bfloat16)
    return (mixed_out, committed)


def solution(mesh):
    return jax.shard_map(
        per_device,
        mesh=mesh,
        in_specs=(
            P(None, "kv"),
            P(),
            P("kv", "tp"),
            P("kv", "tp"),
            P("kv", "tp"),
            P("kv", "tp"),
            P("kv", "tp"),
            P("kv", "tp"),
            P("tp", "kv"),
            P("tp"),
            P(),
            P("kv", "tp", None, None),
            P("kv", None, "tp"),
            P("kv", None, "tp"),
            P("kv", None, "tp"),
            P("kv", None, "tp"),
            P("kv"),
        ),
        out_specs=(P("tp", "kv"), P("kv", "tp", None, None)),
        check_vma=False,
    )
```

profile of v0, /device:TPU:17, one launch (start us, length us, event | category | flops | bytes accessed | tf_op | source)
XLA Modules:
  0.0 226.8 jit_solution(16703975957633322242)
XLA Ops:
  7.3 1.3 fusion.4
  8.6 0.8 dynamic-slice_convert_fusion
  9.4 1.8 convolution_convert_fusion
  11.2 3.3 %convolution_convert_fusion.1 = bf16[1024,1024]{0,1:T(8,128)(2,1)} fusion(bf16[256,1024]{1,0:T(8,128)(2,1)} %param.21, bf16[1024,256]{1,0:T(8,128)(2,1)} %param.17, f32[256]{0:T(256)S(1)} %dynamic-slice_convert_fusion), kind=kOutput, calls=%fused_computation.2 | convolution fusion | flops 538705920 | bytes 3146752 | tf_op jit(solution)/shard_map/dot_general | solution.py:174
  14.5 2.6 %convolution_convert_fusion.2 = bf16[1024,512]{0,1:T(8,128)(2,1)} fusion(bf16[256,512]{1,0:T(8,128)(2,1)} %param.20, bf16[1024,256]{1,0:T(8,128)(2,1)} %param.17, f32[256]{0:T(256)S(1)} %dynamic-slice_convert_fusion), kind=kOutput, calls=%fused_computation.3 | convolution fusion | flops 269746176 | bytes 1836032 | tf_op jit(solution)/shard_map/dot_general | solution.py:174
  17.1 1.5 convolution_convert_fusion.3
  19.0 26.6 %concatenate.9 = bf16[1024,3081]{0,1:T(8,128)(2,1)} concatenate(bf16[1024,512]{0,1:T(8,128)(2,1)} %convolution_convert_fusion.3, bf16[1024,512]{0,1:T(8,128)(2,1)} %convolution_convert_fusion.2, bf16[1024,1024]{0,1:T(8,128)(2,1)} %convolution_convert_fusion.1, bf16[1024,1024]{0,1:T(8,128)(2,1)S(1)} %convolution_convert_fusion, bf16[1024,4]{0,1:T(4,128)(2,1)S(1)} %convolution_convert_fusion.6, ...), dimensions={1} | concatenate | bytes 12619776 | tf_op jit(solution)/shard_map/concatenate | solution.py:14
  45.7 9.4 %copy.339 = bf16[1024,3081]{1,0:T(8,128)(2,1)} copy(bf16[1024,3081]{0,1:T(8,128)(2,1)} %concatenate.9) | data formatting | bytes 12619776
  56.1 82.4 %reduce-scatter.4.cloned.1.call-done = bf16[64,3081]{1,0:T(8,128)(2,1)} async-done(((bf16[1024,3081]{1,0:T(8,128)(2,1)}), bf16[64,3081]{1,0:T(8,128)(2,1)}) %reduce-scatter.4.cloned.1.call-update) | async-done | bytes 394384 | tf_op jit(solution)/shard_map/reduce_scatter | solution.py:15
  138.5 0.9 add_rsqrt_fusion
  139.4 0.9 fusion.106
  140.7 0.6 reduce_window_sum.18
  141.6 0.6 reduce_window_sum.17
  142.6 0.4 fusion.2
  143.0 0.3 fusion.108
  144.7 1.0 divide_multiply_fusion.1
  146.8 0.4 fusion.1
  147.2 0.3 fusion.107
  149.6 0.3 convolution_multiply_fusion.1
  149.9 0.7 multiply_subtract_fusion.2
  150.6 0.4 pad_maximum_fusion
  150.9 10.9 %multiply_add_fusion = f32[16,4,128,256]{3,2,1,0:T(8,128)} fusion(f32[16,4,128,256]{3,2,1,0:T(8,128)} %param.28, f32[16,4]{1,0:T(8,128)S(1)} %copy.283, f32[16,4,4,384]{3,2,1,0:T(4,128)S(1)} %pad_maximum_fusion, f32[16,4,1,384]{3,2,1,0:T(1,128)S(1)} %get-tuple-element.6, f32[16,4,1,384]{3,2,1,0:T(1,128)S(1)} %get-tuple-element.7, ...), kind=kOutput, calls=%fused_computation | convolution fusion | flops 38240256 | bytes 25960448 | tf_op jit(solution)/shard_map/bhcd,bhce->bhde/dot_general | solution.py:83
  161.9 4.0 %fusion.56 = f32[16,4,4,256]{3,2,1,0:T(4,128)S(1)} fusion(f32[16,4,128,256]{3,2,1,0:T(8,128)} %multiply_add_fusion, bf16[16,4,4,128]{3,1,2,0:T(4,128)(2,1)S(1)} %get-tuple-element.16), kind=kOutput, calls=%fused_computation.77 | convolution fusion | flops 16777216 | bytes 8716288 | tf_op jit(solution)/shard_map/bhcd,bhde->bhce/dot_general | solution.py:90
  165.9 0.7 multiply_subtract_fusion
  166.6 0.4 pad_maximum_fusion.1
  167.0 4.2 %fusion = f32[16,4,4,256]{3,2,1,0:T(4,128)S(1)} fusion(bf16[16,4,4,4]{3,2,1,0:T(4,128)(2,1)S(1)} %convolution_multiply_fusion.1, f32[16,4,128,256]{3,2,1,0:T(8,128)} %multiply_add_fusion, f32[16,4,4,384]{3,2,1,0:T(4,128)S(1)} %pad_maximum_fusion.1, f32[16,4,1,384]{3,2,1,0:T(1,128)S(1)} %get-tuple-element.2, f32[16,4,1,384]{3,2,1,0:T(1,128)S(1)} %get-tuple-element.3, ...), kind=kOutput, calls=%fused_computation.9 | convolution fusion | flops 17694720 | bytes 9371648 | tf_op jit(solution)/shard_map/bhcs,bhse->bhce/dot_general | solution.py:91
  171.2 0.3 multiply_reduce_fusion
  171.8 0.5 fusion.10
  172.6 31.5 %all_to_all.10 = bf16[16,64,1024]{2,1,0:T(8,128)(2,1)S(1)} all-to-all(bf16[16,64,1024]{2,1,0:T(8,128)(2,1)S(1)} %broadcast_in_dim.24), channel_id=1, replica_groups=mesh['kv'=16,'tp'=8] {'kv'}, dimensions={0} | all-to-all | bytes 4194304 | tf_op jit(solution)/shard_map/all_to_all | solution.py:25
  204.1 0.7 convolution_convert_fusion.4
  204.8 14.5 %all_to_all.11 = bf16[8,128,256]{2,1,0:T(8,128)(2,1)S(1)} all-to-all(bf16[8,128,256]{2,1,0:T(8,128)(2,1)S(1)} %bitcast.140), channel_id=1, replica_groups=mesh['kv'=16,'tp'=8] {'tp'}, dimensions={0} | all-to-all | bytes 1048576 | tf_op jit(solution)/shard_map/all_to_all | solution.py:47
  219.3 0.7 reduce_sum.62
  (111 shorter events, 7.5 us)
Async XLA Ops:
  7.2 2.2 copy-start
  7.2 9.9 %copy-start.1 = (bf16[1024,256]{1,0:T(8,128)(2,1)S(1)}, bf16[1024,256]{1,0:T(8,128)(2,1)}, u32[]{:S(2)}) copy-start(bf16[1024,256]{1,0:T(8,128)(2,1)} %param.17) | copy-start | bytes 1572868
  7.2 9.9 %copy-start.4 = (bf16[256,512]{1,0:T(8,128)(2,1)S(1)}, bf16[256,512]{1,0:T(8,128)(2,1)}, u32[]{:S(2)}) copy-start(bf16[256,512]{1,0:T(8,128)(2,1)} %param.19) | copy-start | bytes 786436
  7.2 11.3 %copy-start.11 = (bf16[256,4]{0,1:T(4,128)(2,1)S(1)}, bf16[256,4]{0,1:T(4,128)(2,1)}, u32[]{:S(2)}) copy-start(bf16[256,4]{0,1:T(4,128)(2,1)} %param.24) | copy-start | bytes 6148
  7.2 11.6 %copy-start.12 = (bf16[256,4]{0,1:T(4,128)(2,1)S(1)}, bf16[256,4]{0,1:T(4,128)(2,1)}, u32[]{:S(2)}) copy-start(bf16[256,4]{0,1:T(4,128)(2,1)} %param.23) | copy-start | bytes 6148
  7.2 131.2 %reduce-scatter.4.cloned.1.call-start = ((), (), s32[]{:S(2)}) async-start(), calls=%async_computation.3 | async-start | bytes 6963200 | tf_op jit(solution)/shard_map/reduce_scatter | solution.py:15
  45.7 9.4 %copy-start.6 = (f32[16,4,4]{0,2,1:T(4,128)S(1)}, f32[16,4,4]{0,2,1:T(4,128)}, u32[]{:S(2)}) copy-start(f32[16,4,4]{0,2,1:T(4,128)} %param.32) | copy-start | bytes 3076
  45.7 9.5 %copy-start.13 = (f32[4]{0:T(128)S(1)}, f32[4]{0:T(128)}, u32[]{:S(2)}) copy-start(f32[4]{0:T(128)} %param.26) | copy-start | bytes 52
  45.7 9.5 %copy-start.9 = (s32[16]{0:T(128)S(1)}, s32[16]{0:T(128)}, u32[]{:S(2)}) copy-start(s32[16]{0:T(128)} %param.33) | copy-start | bytes 196
  45.7 9.7 %copy-start.7 = (f32[16,4,4]{0,2,1:T(4,128)S(1)}, f32[16,4,4]{0,2,1:T(4,128)}, u32[]{:S(2)}) copy-start(f32[16,4,4]{0,2,1:T(4,128)} %param.31) | copy-start | bytes 3076
  45.7 9.8 %copy-start.2 = (bf16[16,4,512]{2,1,0:T(4,128)(2,1)S(1)}, bf16[16,4,512]{2,1,0:T(4,128)(2,1)}, u32[]{:S(2)}) copy-start(bf16[16,4,512]{2,1,0:T(4,128)(2,1)} %param.29) | copy-start | bytes 196612
  45.7 10.2 %copy-start.5 = (bf16[16,4,1024]{2,1,0:T(4,128)(2,1)S(1)}, bf16[16,4,1024]{2,1,0:T(4,128)(2,1)}, u32[]{:S(2)}) copy-start(bf16[16,4,1024]{2,1,0:T(4,128)(2,1)} %param.30) | copy-start | bytes 393220
  138.5 10.1 %copy-start.3 = (bf16[64,3081]{1,0:T(8,128)(2,1)S(1)}, bf16[64,3081]{1,0:T(8,128)(2,1)}, u32[]{:S(2)}) copy-start(bf16[64,3081]{1,0:T(8,128)(2,1)} %reduce-scatter.4.cloned.1.call-done) | copy-start | bytes 1183108
  161.9 9.9 %copy-start.8 = (f32[256]{0:T(256)S(1)}, f32[256]{0:T(256)}, u32[]{:S(2)}) copy-start(f32[256]{0:T(256)} %param.27) | copy-start | bytes 3076
  167.0 37.1 %copy-start.10 = (bf16[1024,256]{1,0:T(8,128)(2,1)S(1)}, bf16[1024,256]{1,0:T(8,128)(2,1)}, u32[]{:S(2)}) copy-start(bf16[1024,256]{1,0:T(8,128)(2,1)} %param.25) | copy-start | bytes 1572868
Sparse Core Ops, SparseCore 0:
  55.2 83.2 reduce-scatter.3
where the time goes:
time: 231 us; the launch traced here: 227 us
  waiting for transfers between devices  82.4 us (36%)
  blocking collectives  45.9 us (20%)
  local copies, waits for them, and re-layouts  42.3 us (18%)
  matrix products  30.6 us (13%)
  between operations  14.5 us (6%)
  other arithmetic  10.9 us (5%)
    reduce_scatter x1, waiting for transfers between devices, in_one_piece(): lax.psum_scatter(both, axis, scatter_dimension=dim, tiled=True)  82.4 us
    all_to_all x1, blocking collectives, sent_to_all(): return lax.all_to_all(copies, axis, split_axis=0, concat_axis=0, tiled=True)  31.5 us
    concatenate x1, local copies, waits for them, and re-layouts, in_one_piece(): both = jnp.concatenate(columns, axis=along)  26.6 us
    all_to_all x1, blocking collectives, sent_and_summed(): lax.all_to_all(in_blocks(value, dim, count), axis, 0, 0, tiled=True)  14.5 us
    dot_general x1, matrix products, advance(): jnp.einsum('bhcd,bhce->bhde', key_rows * tail_decay[..., None], fresh_val...  10.9 us
    unnamed x34, local copies, waits for them, and re-layouts  9.79 us
    dot_general x6, matrix products, per_device(): jnp.dot(scaled, weight, preferred_element_type=jnp.float32)  9.64 us
  transfers between devices with their start and end apart: 1, of which 1 were waited for; matrix products, arithmetic and copies ran while one was open for 0% of the time, Pallas kernels for 0%

commit v1 on v0

v1 whole, which is shorter than its diff:
```python
import functools

import jax
import jax.numpy as jnp
from jax import lax
from jax.experimental import pallas as pl
from jax.experimental.pallas import tpu as pltpu
from jax.sharding import PartitionSpec as P

MESH = pl.DeviceIdType.MESH
HIGHEST = lax.Precision.HIGHEST
F32 = jnp.float32
BF16 = jnp.bfloat16
norm_eps = 1e-06

TOK = 1024
OWN = 64
SEQ = 16
HD = 4
DK = 128
DV = 256
KB = 256
D = 4096
COLS = 2 * DK + 2 * DV


def softplus(x):
    return jnp.maximum(x, 0.0) + jnp.log1p(jnp.exp(-jnp.abs(x)))


def sigmoid(x):
    return 1.0 / (1.0 + jnp.exp(-x))


def silu(x):
    return x * sigmoid(x)


def place(shape):
    return lax.rem(lax.broadcasted_iota(jnp.int32, shape, 0), 4)


def back(x, j):
    return x if j == 0 else pltpu.roll(x, j, 0)


def ahead(x, j):
    return pltpu.roll(x, x.shape[0] - j, 0)


def wide(col, width):
    return jnp.broadcast_to(col, (col.shape[0], width))


def running_sum(g, at):
    c = g
    for j in (1, 2, 3):
        c = c + jnp.where(at >= j, back(g, j), 0.0)
    return c


def tail_sum(g, at):
    s = jnp.zeros_like(g)
    for j in (1, 2, 3):
        s = s + jnp.where(at + j <= 3, ahead(g, j), 0.0)
    return s


def unit(x):
    return x * lax.rsqrt(jnp.sum(x * x, -1, keepdims=True) + norm_eps)


def decays(c, at):
    out = [jnp.ones_like(c)]
    for j in (1, 2, 3):
        out.append(jnp.where(at >= j, jnp.exp(jnp.where(at >= j, c - back(c, j), 0.0)), 0.0))
    return out


def inverse_rows(k, b, w):
    low = [None]
    for j in (1, 2, 3):
        dots = jnp.sum(k * back(k, j), -1, keepdims=True)
        low.append(b * dots * w[j])
    one, two, three = low[1], low[2], low[3]
    t1 = -one
    t2 = one * back(one, 1) - two
    t3 = one * back(two, 1) + two * back(one, 2) - three - one * back(one, 1) * back(one, 2)
    return t1, t2, t3


def mixed(x, coefs):
    out = x
    for j, coef in enumerate(coefs):
        out = out + coef * back(x, j + 1)
    return out


def dot(a, b):
    return jnp.dot(a, b, preferred_element_type=F32)


def columns_of(rows):
    eye = (
        lax.broadcasted_iota(jnp.int32, (OWN, 128), 0)
        == lax.broadcasted_iota(jnp.int32, (OWN, 128), 1)
    ).astype(F32)
    return lax.dot_general(
        eye, rows, (((1,), (1,)), ((), ())), precision=HIGHEST, preferred_element_type=F32
    )


def pick(cols, at):
    lane = lax.broadcasted_iota(jnp.int32, cols.shape, 1)
    return wide(jnp.sum(jnp.where(lane == at, cols, 0.0), -1, keepdims=True), 128)


def both(x):
    return jnp.concatenate([x, x], 1)


def commit_kernel(small_ref, rate_ref, keys_ref, values_ref, state_ref, out_ref, lhs, ktail, bv, tri, last):
    step = pl.program_id(0)

    @pl.when(step == 0)
    def _():
        at = place((OWN, 128))
        s = small_ref[...]
        row = lax.broadcasted_iota(jnp.int32, (8, 128), 0)
        rate = jnp.zeros((8, 128), F32)
        for h in range(HD):
            rate = jnp.where(row == 4 + h, rate_ref[h], rate)
        taken = s[8:16]
        top = jnp.where(row < 4, sigmoid(s[0:8]), -rate * softplus(s[0:8])) * taken
        cols = columns_of(jnp.concatenate([top, taken], 0))
        for h in range(HD):
            b = wide(cols[:, h : h + 1], 128)
            g = wide(cols[:, 4 + h : 5 + h], 128)
            k = unit(keys_ref[:, h * DK : (h + 1) * DK].astype(F32))
            c = running_sum(g, at)
            tail = tail_sum(g, at)
            w = decays(c, at)
            t1, t2, t3 = inverse_rows(k, b, w)
            tri[h, 0], tri[h, 1], tri[h, 2] = t1, t2, t3
            lhs[h] = b * k * jnp.exp(c)
            ktail[h] = k * jnp.exp(tail)
            bv[h] = both(b) * values_ref[:, h * DV : (h + 1) * DV].astype(F32)
            last[h] = jnp.exp(c + tail)

    rows = pl.ds(pl.multiple_of(step * 8, 8), 8)
    row = lax.broadcasted_iota(jnp.int32, (8, 256), 0)
    row1 = lax.broadcasted_iota(jnp.int32, (8, 128), 0)
    for h in range(HD):
        left = lhs[h, rows, :].astype(BF16)
        s0, s1 = state_ref[0, h], state_ref[1, h]
        z = jnp.where(row < 4, dot(left, s0.astype(BF16)), dot(left, s1.astype(BF16)))
        coefs = [both(tri[h, j, rows, :]) for j in range(3)]
        fresh = mixed(bv[h, rows, :] - z, coefs)
        kt = ktail[h, rows, :]
        kt2 = jnp.concatenate([jnp.where(row1 < 4, kt, 0.0), jnp.where(row1 >= 4, kt, 0.0)], 1)
        upd = lax.dot_general(
            kt2.astype(BF16),
            fresh.astype(BF16),
            (((0,), (0,)), ((), ())),
            preferred_element_type=F32,
        )
        keep = last[h, rows, :]
        out_ref[0, h] = s0 * keep[0:1, 0:1] + upd[0:DK]
        out_ref[1, h] = s1 * keep[4:5, 0:1] + upd[DK:]


def commit(small, rate, keys, values, state):
    whole = lambda *shape: pl.BlockSpec(shape, lambda i: (0,) * len(shape))
    return pl.pallas_call(
        commit_kernel,
        grid=(SEQ // 2,),
        in_specs=[
            whole(16, 128),
            pl.BlockSpec(memory_space=pltpu.SMEM),
            whole(OWN, HD * DK),
            whole(OWN, HD * DV),
            pl.BlockSpec((2, HD, DK, DV), lambda i: (i, 0, 0, 0)),
        ],
        out_specs=pl.BlockSpec((2, HD, DK, DV), lambda i: (i, 0, 0, 0)),
        out_shape=jax.ShapeDtypeStruct((SEQ, HD, DK, DV), F32),
        scratch_shapes=[
            pltpu.VMEM((HD, OWN, 128), F32),
            pltpu.VMEM((HD, OWN, 128), F32),
            pltpu.VMEM((HD, OWN, DV), F32),
            pltpu.VMEM((HD, 3, OWN, 128), F32),
            pltpu.VMEM((HD, OWN, 128), F32),
        ],
        compiler_params=pltpu.CompilerParams(dimension_semantics=("arbitrary",)),
        name="commit",
    )(small, rate, keys, values, state)


class Sems:
    def __init__(self, send, recv):
        self.send, self.recv, self.at = send, recv, 0
        self.sent = []

    def copy(self, src, dst, device):
        n = self.at
        self.at += 1
        return pltpu.make_async_remote_copy(
            src_ref=src,
            dst_ref=dst,
            send_sem=self.send.at[n],
            recv_sem=self.recv.at[n],
            device_id=device,
            device_id_type=MESH,
        )

    def go(self, copy):
        copy.start()
        self.sent.append(copy)


N_SEM = 3 * 2 + 3 * 5 + 3 * 2 + 3 + 3 + 3 + 12 + 12 + 36 + 7
N_LOC = 8


def mix_kernel(
    hidden,
    gain,
    w_query,
    w_key,
    w_value,
    w_gate,
    w_small,
    w_out,
    rate_ref,
    head_gain,
    state,
    out_ref,
    hid,
    scaled,
    wbuf,
    wsm,
    st32,
    st16,
    wo,
    psend,
    precv,
    ssend,
    srecv,
    csend,
    proj,
    gath,
    osend,
    orecv,
    zk_ref,
    zq_ref,
    lhs_ref,
    send,
    recv,
    loc,
):
    kv, tp = lax.axis_index("kv"), lax.axis_index("tp")
    core, y = lax.rem(tp, 2), tp // 2
    z, x = kv // 4, lax.rem(kv, 4)
    a = z + core * (x - z)
    b = x + core * (z - x)
    sa, sb = 4 - 3 * core, 1 + 3 * core

    def kv_at(a_, b_):
        return a_ * sa + b_ * sb

    def turn(i, d):
        return lax.rem(i + d + 4, 4)

    sems = Sems(send, recv)
    head_block = pl.multiple_of(a * DK, 128)

    own_rows = pl.ds(pl.multiple_of(a * KB, 256), KB)
    local = [
        pltpu.make_async_copy(hidden, hid.at[a], loc.at[0]),
        pltpu.make_async_copy(w_small, wsm.at[a], loc.at[1]),
        pltpu.make_async_copy(w_query.at[:, pl.ds(head_block, DK)], wbuf.at[own_rows, pl.ds(0, DK)], loc.at[2]),
        pltpu.make_async_copy(w_key.at[:, pl.ds(head_block, DK)], wbuf.at[own_rows, pl.ds(DK, DK)], loc.at[3]),
        pltpu.make_async_copy(
            w_value.at[:, pl.ds(pl.multiple_of(a * DV, 256), DV)], wbuf.at[own_rows, pl.ds(2 * DK, DV)], loc.at[4]
        ),
        pltpu.make_async_copy(
            w_gate.at[:, pl.ds(pl.multiple_of(a * DV, 256), DV)],
            wbuf.at[own_rows, pl.ds(2 * DK + DV, DV)],
            loc.at[5],
        ),
        pltpu.make_async_copy(state, st32, loc.at[6]),
        pltpu.make_async_copy(w_out, wo, loc.at[7]),
    ]
    for copy in local:
        copy.start()

    barrier = pltpu.get_barrier_semaphore()
    for d in (1, 2, 3):
        pl.semaphore_signal(barrier, inc=1, device_id=(kv_at(turn(a, d), b), tp), device_id_type=MESH)
        pl.semaphore_signal(barrier, inc=1, device_id=(kv_at(a, turn(b, d)), tp), device_id_type=MESH)
    for e in range(1, 8):
        pl.semaphore_signal(barrier, inc=1, device_id=(kv, lax.rem(tp + e, 8)), device_id_type=MESH)
    pl.semaphore_wait(barrier, 13)

    def quarter(i):
        return pl.ds(pl.multiple_of(i * 256, 256), 256)

    hid_in = {}
    for d in (2, 1, 3):
        peer = (kv_at(turn(a, d), b), tp)
        for e in (0, 2):
            rows = quarter(turn(y, e))
            copy = sems.copy(hidden.at[rows, :], hid.at[a, rows, :], peer)
            sems.go(copy)
            hid_in[d, e] = copy
    w_in = {}
    for d in (2, 1, 3):
        to = turn(a, d)
        peer = (kv_at(to, b), tp)
        cols = pl.ds(pl.multiple_of(to * DK, 128), DK)
        cols2 = pl.ds(pl.multiple_of(to * DV, 256), DV)
        w_in[d] = [
            sems.copy(w_query.at[:, cols], wbuf.at[own_rows, pl.ds(0, DK)], peer),
            sems.copy(w_key.at[:, cols], wbuf.at[own_rows, pl.ds(DK, DK)], peer),
            sems.copy(w_value.at[:, cols2], wbuf.at[own_rows, pl.ds(2 * DK, DV)], peer),
            sems.copy(w_gate.at[:, cols2], wbuf.at[own_rows, pl.ds(2 * DK + DV, DV)], peer),
            sems.copy(w_small, wsm.at[a], peer),
        ]
        for copy in w_in[d]:
            sems.go(copy)

    def scale_block(slot):
        weight = gain[kv_at(slot, b)]

        def body(n, _):
            kb, ka = n // 4, lax.rem(n, 4)
            rows = pl.ds(pl.multiple_of(kv_at(ka, kb) * OWN, OWN), OWN)
            to = pl.ds(pl.multiple_of(n * OWN, OWN), OWN)
            block = hid[slot, rows, :].astype(F32) * weight
            scaled[to, pl.ds(pl.multiple_of(slot * KB, 256), KB)] = block.astype(BF16)
            return 0

        lax.fori_loop(0, 16, body, 0)

    local[0].wait()
    scale_block(a)
    y_in = {}
    for d in (1, 3, 2):
        hid_in[d, 0].wait_recv()
        slot = turn(a, -d)
        rows = quarter(y)
        y_in[d] = []
        for e in (1, 3):
            peer = (kv, 2 * turn(y, e) + core)
            copy = sems.copy(hid.at[slot, rows, :], hid.at[slot, rows, :], peer)
            sems.go(copy)
            y_in[d].append(copy)

    local[6].wait()

    def round_states(n, _):
        st16[n] = st32[n].astype(BF16)
        return 0

    lax.fori_loop(0, SEQ, round_states, 0)

    for d in (1, 3, 2):
        hid_in[d, 2].wait_recv()
        for copy in y_in[d]:
            copy.wait_recv()
        scale_block(turn(a, -d))

    for n in (1, 2, 3, 4, 5):
        local[n].wait()
    for d in (1, 3, 2):
        for copy in w_in[d]:
            copy.wait_recv()

    weights = wbuf[...]
    ones = jnp.ones((8, 4 * KB), BF16)
    small_w = jnp.concatenate([wsm[i] for i in range(4)], 1).astype(BF16)
    s_in, p_in = {}, {}
    for d in (2, 1, 3, 0):
        to = turn(b, d)
        peer = (kv_at(a, to), tp)
        rows = pl.ds(pl.multiple_of(to * 256, 256), 256)
        psend[d] = dot(scaled[rows, :], weights).astype(BF16)
        if d:
            copy = sems.copy(psend.at[d], precv.at[d - 1], peer)
            sems.go(copy)
            p_in[d] = copy
    for d in (2, 1, 3, 0):
        to = turn(b, d)
        peer = (kv_at(a, to), tp)
        mine = pl.ds(pl.multiple_of(to * 256 + a * OWN, OWN), OWN)
        token = pl.ds(pl.multiple_of(kv_at(a, to) * OWN, OWN), OWN)
        nt = (((1,), (1,)), ((), ()))
        part = lax.dot_general(small_w, scaled[mine, :], nt, preferred_element_type=F32)
        square = jnp.zeros((8, OWN), F32)
        for i in range(4):
            h32 = hid[i, token, :].astype(F32)
            sq = h32 * h32
            high = sq.astype(BF16)
            low = (sq - high.astype(F32)).astype(BF16)
            square = square + lax.dot_general(ones[:, :KB], high, nt, preferred_element_type=F32)
            square = square + lax.dot_general(ones[:, :KB], low, nt, preferred_element_type=F32)
        ssend[d] = jnp.concatenate([jnp.concatenate([part, square], 0), jnp.zeros((16, 64), F32)], 1)
        if d:
            copy = sems.copy(ssend.at[d], srecv.at[d - 1], peer)
            sems.go(copy)
            s_in[d] = copy

    for d in (1, 3, 2):
        p_in[d].wait_recv()
    c_in = {}
    for d in (2, 1, 3, 0):
        to = turn(a, d)
        rows = pl.ds(pl.multiple_of(to * OWN, OWN), OWN)
        total = psend[0, rows, :].astype(F32)
        for i in range(3):
            total = total + precv[i, rows, :].astype(F32)
        if d:
            csend[d - 1] = total.astype(BF16)
            copy = sems.copy(csend.at[d - 1], proj.at[a], (kv_at(to, b), tp))
            sems.go(copy)
            c_in[d] = copy
        else:
            proj[a] = total.astype(BF16)

    for d in (1, 3, 2):
        s_in[d].wait_recv()
    small = ssend[0]
    for i in range(3):
        small = small + srecv[i]
    inv = lax.rsqrt(small[8:16] / D + norm_eps)
    row = lax.broadcasted_iota(jnp.int32, (8, 128), 0)
    rate = jnp.zeros((8, 128), F32)
    for h in range(HD):
        rate = jnp.where(row == 4 + h, rate_ref[h], rate)
    pre = small[0:8] * inv
    top = jnp.where(row < 4, sigmoid(pre), -rate * softplus(pre))
    cols = columns_of(jnp.concatenate([top, inv], 0))
    inv_col = cols[:, 8:9]
    at = place((OWN, 128))
    row4 = lax.broadcasted_iota(jnp.int32, (8, DV), 0)

    first_in, peer_in = {}, {}
    for d in range(4):
        h = turn(a, -d)
        if d:
            c_in[d].wait_recv()
        bcol = pick(cols, h)
        c = running_sum(pick(cols, h + 4), at)
        w = decays(c, at)
        grow = jnp.exp(c)
        q = unit(silu(proj[h, :, 0:DK].astype(F32) * inv_col)) * DK ** (-0.5)
        k = unit(silu(proj[h, :, DK : 2 * DK].astype(F32) * inv_col))
        v = silu(proj[h, :, 2 * DK : 2 * DK + DV].astype(F32) * inv_col)
        coefs = [both(t) for t in inverse_rows(k, bcol, w)]
        scores = [both(wide(jnp.sum(q * back(k, j), -1, keepdims=True), 128) * w[j]) for j in range(4)]
        kl = bcol * k * grow
        ql = q * grow
        for i in range(SEQ // 2):
            rows = slice(8 * i, 8 * i + 8)
            left = jnp.concatenate([kl[rows], ql[rows]], 0).astype(BF16)
            z0 = dot(left, st16[2 * i, h])
            z1 = dot(left, st16[2 * i + 1, h])
            zk_ref[rows, :] = jnp.where(row4 < 4, z0[0:8], z1[0:8])
            zq_ref[rows, :] = jnp.where(row4 < 4, z0[8:16], z1[8:16])
        fresh = mixed(both(bcol) * v - zk_ref[...], coefs)
        res = zq_ref[...]
        for j in range(4):
            res = res + scores[j] * back(fresh, j)
        norm = res * lax.rsqrt(jnp.mean(res * res, -1, keepdims=True) + norm_eps) * head_gain[...]
        gate = silu(proj[h, :, 2 * DK + DV :].astype(F32) * inv_col)
        gath[kv, h] = (norm * gate).astype(BF16)
        for e in (2, 1, 3):
            copy = sems.copy(gath.at[kv, h], gath.at[kv, h], (kv_at(a, turn(b, e)), tp))
            sems.go(copy)
            peer_in[e, d] = copy
            copy = sems.copy(gath.at[kv, h], gath.at[kv, h], (kv_at(turn(a, e), b), tp))
            sems.go(copy)
            first_in[e, d] = copy

    on_in = []
    for d in range(4):
        for e in (1, 3, 2):
            first_in[e, d].wait_recv()
            src = turn(a, -e)
            h = turn(src, -d)
            block = gath.at[kv_at(src, b), h]
            for f in (2, 1, 3):
                copy = sems.copy(block, block, (kv_at(a, turn(b, f)), tp))
                sems.go(copy)
                on_in.append(copy)
    for copy in peer_in.values():
        copy.wait_recv()
    for copy in on_in:
        copy.wait_recv()

    local[7].wait()
    o_in = {}
    for e in (4, 5, 2, 3, 6, 7, 1, 0):
        to = lax.rem(tp + e, 8)
        total = None
        for h in range(HD):
            part = jnp.concatenate([gath[2 * to, h], gath[2 * to + 1, h]], 0)
            term = dot(part, wo[h * DV : (h + 1) * DV, :])
            total = term if total is None else total + term
        osend[e] = total.astype(BF16)
        if e:
            copy = sems.copy(osend.at[e], orecv.at[e - 1], (kv, to))
            sems.go(copy)
            o_in[e] = copy
    for e in range(1, 8):
        o_in[e].wait_recv()
    total = osend[0].astype(F32)
    for i in range(7):
        total = total + orecv[i].astype(F32)
    out_ref[...] = total.astype(BF16)
    for copy in sems.sent:
        copy.wait_send()
    assert sems.at == N_SEM, sems.at


def mix(hidden, gain, w_query, w_key, w_value, w_gate, w_small, w_out, rate, head_gain, state):
    hbm = pl.BlockSpec(memory_space=pl.ANY)
    vmem = pl.BlockSpec(memory_space=pltpu.VMEM)
    return pl.pallas_call(
        mix_kernel,
        in_specs=[hbm, vmem, hbm, hbm, hbm, hbm, hbm, hbm, pl.BlockSpec(memory_space=pltpu.SMEM), vmem, hbm],
        out_specs=vmem,
        out_shape=jax.ShapeDtypeStruct((128, 256), BF16),
        scratch_shapes=[
            pltpu.VMEM((4, TOK, KB), BF16),
            pltpu.VMEM((TOK, 4 * KB), BF16),
            pltpu.VMEM((4 * KB, COLS), BF16),
            pltpu.VMEM((4, 8, KB), F32),
            pltpu.VMEM((SEQ, HD, DK, DV), F32),
            pltpu.VMEM((SEQ, HD, DK, DV), BF16),
            pltpu.VMEM((HD * DV, 256), BF16),
            pltpu.VMEM((4, 256, COLS), BF16),
            pltpu.VMEM((3, 256, COLS), BF16),
            pltpu.VMEM((4, 16, 128), F32),
            pltpu.VMEM((3, 16, 128), F32),
            pltpu.VMEM((3, OWN, COLS), BF16),
            pltpu.VMEM((HD, OWN, COLS), BF16),
            pltpu.VMEM((16, HD, OWN, DV), BF16),
            pltpu.VMEM((8, 128, 256), BF16),
            pltpu.VMEM((7, 128, 256), BF16),
            pltpu.VMEM((OWN, DV), F32),
            pltpu.VMEM((OWN, DV), F32),
            pltpu.VMEM((OWN, DK), F32),
            pltpu.SemaphoreType.DMA((N_SEM,)),
            pltpu.SemaphoreType.DMA((N_SEM,)),
            pltpu.SemaphoreType.DMA((N_LOC,)),
        ],
        compiler_params=pltpu.CompilerParams(
            collective_id=0, has_side_effects=True, vmem_limit_bytes=60 * 1024 * 1024
        ),
        name="mix",
    )(hidden, gain, w_query, w_key, w_value, w_gate, w_small, w_out, rate, head_gain, state)


def per_device(
    hidden,
    norm_gain,
    w_query,
    w_key,
    w_value,
    w_gate,
    w_write,
    w_decay,
    w_out,
    decay_rate,
    head_gain,
    carried_state,
    last_keys,
    last_values,
    last_writes,
    last_decays,
    accepted,
):
    def rows_of(small):
        return jnp.transpose(small, (2, 0, 1)).reshape(HD, OWN)

    taken = (jnp.arange(4, dtype=jnp.int32)[None, :] < accepted[:, None]).astype(F32).reshape(1, OWN)
    small = jnp.concatenate(
        [rows_of(last_writes), rows_of(last_decays), jnp.broadcast_to(taken, (8, OWN))], 0
    )
    small = jnp.pad(small, ((0, 0), (0, 128 - OWN)))
    committed = commit(
        small,
        decay_rate,
        last_keys.reshape(OWN, HD * DK),
        last_values.reshape(OWN, HD * DV),
        carried_state,
    )
    w_small = jnp.concatenate([w_write.T, w_decay.T], 0).astype(F32)
    mixed_out = mix(
        hidden,
        norm_gain.astype(F32).reshape(16, 1, 256),
        w_query,
        w_key,
        w_value,
        w_gate,
        w_small,
        w_out,
        decay_rate,
        head_gain.reshape(1, DV),
        committed,
    )
    return (mixed_out, committed)


def solution(mesh):
    return jax.shard_map(
        per_device,
        mesh=mesh,
        in_specs=(
            P(None, "kv"),
            P(),
            P("kv", "tp"),
            P("kv", "tp"),
            P("kv", "tp"),
            P("kv", "tp"),
            P("kv", "tp"),
            P("kv", "tp"),
            P("tp", "kv"),
            P("tp"),
            P(),
            P("kv", "tp", None, None),
            P("kv", None, "tp"),
            P("kv", None, "tp"),
            P("kv", None, "tp"),
            P("kv", None, "tp"),
            P("kv"),
        ),
        out_specs=(P("tp", "kv"), P("kv", "tp", None, None)),
        check_vma=False,
    )
```

time: 231 us -> 90.2 us (0.39)
  the two profiles are of different devices: /device:TPU:17 before, /device:TPU:1 now
where the time goes in v1:
time: 90.2 us; the launch traced here: 89.6 us
  Pallas kernels  80 us (89%)
  local copies, waits for them, and re-layouts  6.41 us (7%)
  other arithmetic  2.55 us (3%)
    pallas_call x1, Pallas kernels, mix(): pl.pallas_call(mix_kernel, in_specs=[hbm, vmem, hbm, hbm, hbm, hbm, hbm,...  68.5 us
    pallas_call x1, Pallas kernels, commit(): pl.pallas_call(commit_kernel, grid=(SEQ // 2,), in_specs=[whole(16, 128),...  11.5 us

profile of v1, /device:TPU:1, one launch (start us, length us, event | category | flops | bytes accessed | tf_op | source)
XLA Modules:
  0.0 89.6 jit_solution(13849102891230679818)
XLA Ops:
  0.6 1.6 %reshape.49.values_ref = bf16[64,1024]{1,0:T(8,128)(2,1)} reshape(bf16[16,4,1024]{2,1,0:T(4,128)(2,1)} %param.30) | data formatting | bytes 262144 | tf_op jit(solution)/shard_map/reshape | solution.py:595
  2.2 0.8 copy.21
  3.0 0.1 reshape.46
  3.1 0.8 copy.22
  3.9 0.1 reshape.47
  4.0 0.7 fusion
  4.7 0.1 reshape.52
  4.8 0.6 select_maximum_fusion.small_ref
  5.4 1.5 %reshape.48.keys_ref = bf16[64,512]{1,0:T(8,128)(2,1)} reshape(bf16[16,4,512]{2,1,0:T(4,128)(2,1)} %param.29) | data formatting | bytes 131072 | tf_op jit(solution)/shard_map/reshape | solution.py:594
  6.9 0.0 copy-start
  6.9 0.0 copy-start.1
  6.9 0.0 copy-start.2
  6.9 11.5 %commit.1.state = f32[16,4,128,256]{3,2,1,0:T(8,128)} custom-call(f32[16,128]{1,0:T(8,128)} %select_maximum_fusion.small_ref, f32[4]{0:T(128)} %rate_ref.3, bf16[64,512]{1,0:T(8,128)(2,1)} %reshape.48.keys_ref, bf16[64,1024]{1,0:T(8,128)(2,1)} %reshape.49.values_ref, f32[16,4,128,256]{3,2,1,0:T(8,128)} %state_ref.1), custom_call_target="tpu_custom_call" | custom-call | tf_op jit(solution)/shard_map/commit/pallas_call | solution.py:174
  18.4 0.0 copy-done
  18.4 0.6 reshape.50
  19.0 0.0 copy-done.1
  19.0 0.0 copy-done.2
  19.0 0.6 maximum_convert_fusion.w_small
  19.6 68.5 %mix.1 = bf16[128,256]{1,0:T(8,128)(2,1)} custom-call(bf16[1024,256]{1,0:T(8,128)(2,1)} %hidden.1, f32[16,1,256]{2,1,0:T(1,128)} %bitcast.6, bf16[256,512]{1,0:T(8,128)(2,1)} %w_query.1, bf16[256,512]{1,0:T(8,128)(2,1)} %w_key.1, bf16[256,1024]{1,0:T(8,128)(2,1)} %w_value.1, bf16[256,1024]{1,0:T(8,128)(2,1)} %w_gate.1, ...), custom_call_target="tpu_custom_call" | custom-call | tf_op jit(solution)/shard_map/mix/pallas_call | solution.py:528
  88.1 1.5 %copy.24 = bf16[128,256]{1,0:T(8,128)(2,1)} copy(bf16[128,256]{1,0:T(8,128)(2,1)} %mix.1) | data formatting | bytes 131072
  (1 shorter events, 0.0 us)
Async XLA Ops:
  6.9 11.5 %copy-start = (bf16[4096]{0:T(1024)(128)(2,1)S(1)}, bf16[4096]{0:T(1024)(128)(2,1)}, u32[]{:S(2)}) copy-start(bf16[4096]{0:T(1024)(128)(2,1)} %param.18) | copy-start | bytes 24580
  6.9 12.1 %copy-start.1 = (bf16[256,4]{0,1:T(4,128)(2,1)S(1)}, bf16[256,4]{0,1:T(4,128)(2,1)}, u32[]{:S(2)}) copy-start(bf16[256,4]{0,1:T(4,128)(2,1)} %param.24) | copy-start | bytes 6148
  6.9 12.1 %copy-start.2 = (bf16[256,4]{0,1:T(4,128)(2,1)S(1)}, bf16[256,4]{0,1:T(4,128)(2,1)}, u32[]{:S(2)}) copy-start(bf16[256,4]{0,1:T(4,128)(2,1)} %param.23) | copy-start | bytes 6148

commit v2 on v1

v2 whole, which is shorter than its diff:
```python
import functools

import jax
import jax.numpy as jnp
from jax import lax
from jax.experimental import pallas as pl
from jax.experimental.pallas import tpu as pltpu
from jax.sharding import PartitionSpec as P

MESH = pl.DeviceIdType.MESH
HIGHEST = lax.Precision.HIGHEST
F32 = jnp.float32
BF16 = jnp.bfloat16
norm_eps = 1e-06

TOK = 1024
OWN = 64
SEQ = 16
HD = 4
DK = 128
DV = 256
KB = 256
D = 4096
COLS = 2 * DK + 2 * DV


def softplus(x):
    return jnp.maximum(x, 0.0) + jnp.log1p(jnp.exp(-jnp.abs(x)))


def sigmoid(x):
    return 1.0 / (1.0 + jnp.exp(-x))


def silu(x):
    return x * sigmoid(x)


def place(shape):
    return lax.rem(lax.broadcasted_iota(jnp.int32, shape, 0), 4)


def back(x, j):
    return x if j == 0 else pltpu.roll(x, j, 0)


def ahead(x, j):
    return pltpu.roll(x, x.shape[0] - j, 0)


def wide(col, width):
    return jnp.broadcast_to(col, (col.shape[0], width))


def running_sum(g, at):
    c = g
    for j in (1, 2, 3):
        c = c + jnp.where(at >= j, back(g, j), 0.0)
    return c


def tail_sum(g, at):
    s = jnp.zeros_like(g)
    for j in (1, 2, 3):
        s = s + jnp.where(at + j <= 3, ahead(g, j), 0.0)
    return s


def unit(x):
    return x * lax.rsqrt(jnp.sum(x * x, -1, keepdims=True) + norm_eps)


def decays(c, at):
    out = [jnp.ones_like(c)]
    for j in (1, 2, 3):
        out.append(jnp.where(at >= j, jnp.exp(jnp.where(at >= j, c - back(c, j), 0.0)), 0.0))
    return out


def inverse_rows(k, b, w):
    low = [None]
    for j in (1, 2, 3):
        dots = jnp.sum(k * back(k, j), -1, keepdims=True)
        low.append(b * dots * w[j])
    one, two, three = low[1], low[2], low[3]
    t1 = -one
    t2 = one * back(one, 1) - two
    t3 = one * back(two, 1) + two * back(one, 2) - three - one * back(one, 1) * back(one, 2)
    return t1, t2, t3


def mixed(x, coefs):
    out = x
    for j, coef in enumerate(coefs):
        out = out + coef * back(x, j + 1)
    return out


def dot(a, b):
    return jnp.dot(a, b, preferred_element_type=F32)


def columns_of(rows):
    eye = (
        lax.broadcasted_iota(jnp.int32, (OWN, 128), 0)
        == lax.broadcasted_iota(jnp.int32, (OWN, 128), 1)
    ).astype(F32)
    return lax.dot_general(
        eye, rows, (((1,), (1,)), ((), ())), precision=HIGHEST, preferred_element_type=F32
    )


def pick(cols, at):
    lane = lax.broadcasted_iota(jnp.int32, cols.shape, 1)
    return wide(jnp.sum(jnp.where(lane == at, cols, 0.0), -1, keepdims=True), 128)


def both(x):
    return jnp.concatenate([x, x], 1)


class Sems:
    def __init__(self, send, recv):
        self.send, self.recv, self.at = send, recv, 0
        self.sent = []

    def go(self, src, dst, device):
        n = self.at
        self.at += 1
        copy = pltpu.make_async_remote_copy(
            src_ref=src,
            dst_ref=dst,
            send_sem=self.send.at[n],
            recv_sem=self.recv.at[n],
            device_id=device,
            device_id_type=MESH,
        )
        copy.start()
        self.sent.append(copy)
        return copy


N_SEM = 6 + 3 * 6 + 6 + 9 + 3 + 9 + 12 + 12 + 36
NT = (((1,), (1,)), ((), ()))


def kernel(
    hidden,
    gain,
    w_query,
    w_key,
    w_value,
    w_gate,
    w_write,
    w_decay,
    w_out,
    rate_ref,
    head_gain,
    state,
    last_keys,
    last_values,
    last_writes,
    last_decays,
    accepted,
    out_ref,
    st32,
    hid,
    scaled,
    wbuf,
    wsm,
    st16,
    wo,
    lhs,
    ktail,
    bv,
    tri,
    last,
    psend,
    precv,
    ssend,
    srecv,
    csend,
    proj,
    coef,
    zk,
    zq,
    gath,
    osend,
    orecv,
    send,
    recv,
    loc,
    o_send,
    o_recv,
):
    kv, tp = lax.axis_index("kv"), lax.axis_index("tp")
    core, y = lax.rem(tp, 2), tp // 2
    z, x = kv // 4, lax.rem(kv, 4)
    a = z + core * (x - z)
    b = x + core * (z - x)
    sa, sb = 4 - 3 * core, 1 + 3 * core

    def kv_at(a_, b_):
        return a_ * sa + b_ * sb

    def turn(i, d):
        return lax.rem(i + d + 4, 4)

    def head_cols(h, width):
        return pl.ds(pl.multiple_of(h * width, width), width)

    sems = Sems(send, recv)
    own_rows = pl.ds(pl.multiple_of(a * KB, 256), KB)

    def weight_parts(h):
        return [
            (w_query.at[:, head_cols(h, DK)], wbuf.at[0, own_rows, pl.ds(0, DK)]),
            (w_key.at[:, head_cols(h, DK)], wbuf.at[0, own_rows, pl.ds(DK, DK)]),
            (w_write, wsm.at[a, 0]),
            (w_decay, wsm.at[a, 1]),
            (w_value.at[:, head_cols(h, DV)], wbuf.at[1, own_rows, :]),
            (w_gate.at[:, head_cols(h, DV)], wbuf.at[2, own_rows, :]),
        ]

    pairs = [(hidden, hid.at[a]), (state, st32), (w_out, wo)] + weight_parts(a)
    local = [pltpu.make_async_copy(src, dst, loc.at[n]) for n, (src, dst) in enumerate(pairs)]
    for copy in local:
        copy.start()

    barrier = pltpu.get_barrier_semaphore()
    for d in (1, 2, 3):
        pl.semaphore_signal(barrier, inc=1, device_id=(kv_at(turn(a, d), b), tp), device_id_type=MESH)
        pl.semaphore_signal(barrier, inc=1, device_id=(kv_at(a, turn(b, d)), tp), device_id_type=MESH)
    for e in range(1, 8):
        pl.semaphore_signal(barrier, inc=1, device_id=(kv, lax.rem(tp + e, 8)), device_id_type=MESH)
    pl.semaphore_wait(barrier, 13)

    def quarter(i):
        return pl.ds(pl.multiple_of(i * 256, 256), 256)

    hid_in = {}
    for e in (0, 2):
        for d in (1, 3, 2):
            rows = quarter(turn(y, e))
            hid_in[d, e] = sems.go(hidden.at[rows, :], hid.at[a, rows, :], (kv_at(turn(a, d), b), tp))
    w_in = {d: [] for d in (1, 2, 3)}
    for first, past in ((0, 4), (4, 5), (5, 6)):
        for d in (2, 1, 3):
            to = turn(a, d)
            for src, dst in weight_parts(to)[first:past]:
                w_in[d].append(sems.go(src, dst, (kv_at(to, b), tp)))

    at = place((OWN, 128))
    which = lax.broadcasted_iota(jnp.int32, (OWN, SEQ), 0)
    seq = lax.broadcasted_iota(jnp.int32, (OWN, SEQ), 1)
    raw = jnp.zeros((OWN, 8), F32)
    for p in range(4):
        raw = raw + lax.dot_general(
            (which == 4 * seq + p).astype(F32),
            jnp.concatenate([last_writes[p], last_decays[p]], 0),
            NT,
            precision=HIGHEST,
            preferred_element_type=F32,
        )
    count = jnp.sum(jnp.where(which // 4 == seq, accepted[...].astype(F32), 0.0), -1, keepdims=True)
    taken = (place((OWN, 8)).astype(F32) < count).astype(F32)
    lane8 = lax.broadcasted_iota(jnp.int32, (OWN, 8), 1)
    rate = jnp.zeros((OWN, 8), F32)
    for h in range(HD):
        rate = jnp.where(lane8 == 4 + h, rate_ref[h], rate)
    cols = jnp.where(lane8 < 4, sigmoid(raw), -rate * softplus(raw)) * taken

    for n in range(SEQ // 2):
        rows = slice(8 * n, 8 * n + 8)
        lhs_pair = [last_keys[2 * n + i].astype(F32) for i in (0, 1)]
        val_pair = [last_values[2 * n + i].astype(F32) for i in (0, 1)]
        for h in range(HD):
            cut = slice(h * DK, (h + 1) * DK)
            lhs[h, rows, :] = jnp.concatenate([v[:, cut] for v in lhs_pair], 0)
            cut = slice(h * DV, (h + 1) * DV)
            bv[h, rows, :] = jnp.concatenate([v[:, cut] for v in val_pair], 0)

    def old_head(h, _):
        bcol, g = pick(cols, h), pick(cols, h + 4)
        k = unit(lhs[h])
        c = running_sum(g, at)
        tail = tail_sum(g, at)
        t1, t2, t3 = inverse_rows(k, bcol, decays(c, at))
        tri[h, 0], tri[h, 1], tri[h, 2] = t1, t2, t3
        lhs[h] = bcol * k * jnp.exp(c)
        ktail[h] = k * jnp.exp(tail)
        bv[h] = both(bcol) * bv[h]
        last[h] = jnp.exp(c + tail)
        return 0

    lax.fori_loop(0, HD, old_head, 0)

    y_in = {}
    for d in (1, 3, 2):
        hid_in[d, 0].wait_recv()
        slot = turn(a, -d)
        rows = quarter(y)
        y_in[d] = [
            sems.go(hid.at[slot, rows, :], hid.at[slot, rows, :], (kv, 2 * turn(y, e) + core)) for e in (1, 3)
        ]

    local[1].wait()
    row8 = lax.broadcasted_iota(jnp.int32, (8, DV), 0)
    row8k = lax.broadcasted_iota(jnp.int32, (8, DK), 0)

    def old_pair(n, _):
        rows = pl.ds(pl.multiple_of(n * 8, 8), 8)
        for h in range(HD):
            left = lhs[h, rows, :].astype(BF16)
            s0, s1 = st32[2 * n, h], st32[2 * n + 1, h]
            zz = jnp.where(row8 < 4, dot(left, s0.astype(BF16)), dot(left, s1.astype(BF16)))
            fresh = mixed(bv[h, rows, :] - zz, [both(tri[h, j, rows, :]) for j in range(3)])
            kt = ktail[h, rows, :]
            kt2 = jnp.concatenate([jnp.where(row8k < 4, kt, 0.0), jnp.where(row8k >= 4, kt, 0.0)], 1)
            upd = lax.dot_general(
                kt2.astype(BF16), fresh.astype(BF16), (((0,), (0,)), ((), ())), preferred_element_type=F32
            )
            keep = last[h, rows, :]
            n0 = s0 * keep[0:1, 0:1] + upd[0:DK]
            n1 = s1 * keep[4:5, 0:1] + upd[DK:]
            st32[2 * n, h], st32[2 * n + 1, h] = n0, n1
            st16[2 * n, h], st16[2 * n + 1, h] = n0.astype(BF16), n1.astype(BF16)
        return 0

    lax.fori_loop(0, SEQ // 2, old_pair, 0)

    def scale_block(slot):
        weight = gain[kv_at(slot, b)]

        def body(n, _):
            kb, ka = n // 4, lax.rem(n, 4)
            rows = pl.ds(pl.multiple_of(kv_at(ka, kb) * OWN, OWN), OWN)
            to = pl.ds(pl.multiple_of(n * OWN, OWN), OWN)
            block = hid[slot, rows, :].astype(F32) * weight
            scaled[to, pl.ds(pl.multiple_of(slot * KB, 256), KB)] = block.astype(BF16)
            return 0

        lax.fori_loop(0, 16, body, 0)

    local[0].wait()
    scale_block(a)
    for d in (1, 3, 2):
        hid_in[d, 2].wait_recv()
        for copy in y_in[d]:
            copy.wait_recv()
        scale_block(turn(a, -d))

    p_in, c_in = {}, {}

    def send_parts(chunk, first, past):
        for copy in local[3 + first : 3 + past]:
            copy.wait()
        for d in (1, 3, 2):
            for copy in w_in[d][first:past]:
                copy.wait_recv()
        weights = wbuf[chunk]
        for d in (2, 1, 3, 0):
            to = turn(b, d)
            psend[chunk, d] = dot(scaled[quarter(to), :], weights).astype(BF16)
            if d:
                p_in[chunk, d] = sems.go(
                    psend.at[chunk, d], precv.at[chunk, d - 1], (kv_at(a, to), tp)
                )

    def send_sums(chunk):
        for d in (1, 3, 2):
            p_in[chunk, d].wait_recv()
        for d in (2, 1, 3, 0):
            to = turn(a, d)
            rows = pl.ds(pl.multiple_of(to * OWN, OWN), OWN)
            total = psend[chunk, 0, rows, :].astype(F32)
            for i in range(3):
                total = total + precv[chunk, i, rows, :].astype(F32)
            if d:
                csend[chunk, d - 1] = total.astype(BF16)
                c_in[chunk, d] = sems.go(csend.at[chunk, d - 1], proj.at[chunk, a], (kv_at(to, b), tp))
            else:
                proj[chunk, a] = total.astype(BF16)

    send_parts(0, 0, 4)
    s_in = {}
    ones = jnp.ones((8, KB), BF16)
    for d in (2, 1, 3, 0):
        to = turn(b, d)
        token = pl.ds(pl.multiple_of(kv_at(a, to) * OWN, OWN), OWN)
        mine = pl.ds(pl.multiple_of(to * 256 + a * OWN, OWN), OWN)
        write, decay = jnp.zeros((4, OWN), F32), jnp.zeros((4, OWN), F32)
        square = jnp.zeros((8, OWN), F32)
        for i in range(4):
            rows_i = scaled[mine, i * KB : (i + 1) * KB]
            write = write + lax.dot_general(wsm[i, 0], rows_i, NT, preferred_element_type=F32)
            decay = decay + lax.dot_general(wsm[i, 1], rows_i, NT, preferred_element_type=F32)
            h32 = hid[i, token, :].astype(F32)
            sq = h32 * h32
            high = sq.astype(BF16)
            low = (sq - high.astype(F32)).astype(BF16)
            square = square + lax.dot_general(ones, high, NT, preferred_element_type=F32)
            square = square + lax.dot_general(ones, low, NT, preferred_element_type=F32)
        part = jnp.concatenate([write, decay, square], 0)
        ssend[d] = jnp.concatenate([part, jnp.zeros((16, 64), F32)], 1)
        if d:
            s_in[d] = sems.go(ssend.at[d], srecv.at[d - 1], (kv_at(a, to), tp))
    send_parts(1, 4, 5)
    send_sums(0)
    send_parts(2, 5, 6)

    for d in (1, 3, 2):
        s_in[d].wait_recv()
    small = ssend[0]
    for i in range(3):
        small = small + srecv[i]
    inv = lax.rsqrt(small[8:16] / D + norm_eps)
    row = lax.broadcasted_iota(jnp.int32, (8, 128), 0)
    rate = jnp.zeros((8, 128), F32)
    for h in range(HD):
        rate = jnp.where(row == 4 + h, rate_ref[h], rate)
    pre = small[0:8] * inv
    top = jnp.where(row < 4, sigmoid(pre), -rate * softplus(pre))
    cols = columns_of(jnp.concatenate([top, inv], 0))
    inv_col = cols[:, 8:9]
    send_sums(1)

    def new_keys(d):
        h = turn(a, -d)
        if d:
            c_in[0, d].wait_recv()
        bcol = pick(cols, h)
        c = running_sum(pick(cols, h + 4), at)
        w = decays(c, at)
        grow = jnp.exp(c)
        q = unit(silu(proj[0, h, :, 0:DK].astype(F32) * inv_col)) * DK ** (-0.5)
        k = unit(silu(proj[0, h, :, DK : 2 * DK].astype(F32) * inv_col))
        kl, ql = bcol * k * grow, q * grow
        for i in range(SEQ // 2):
            rows = slice(8 * i, 8 * i + 8)
            left = jnp.concatenate([kl[rows], ql[rows]], 0).astype(BF16)
            z0 = dot(left, st16[2 * i, h])
            z1 = dot(left, st16[2 * i + 1, h])
            zk[d, rows, :] = jnp.where(row8 < 4, z0[0:8], z1[0:8])
            zq[d, rows, :] = jnp.where(row8 < 4, z0[8:16], z1[8:16])
        t1, t2, t3 = inverse_rows(k, bcol, w)
        coef[d, 0], coef[d, 1], coef[d, 2] = t1, t2, t3
        for j in range(4):
            coef[d, 3 + j] = wide(jnp.sum(q * back(k, j), -1, keepdims=True), 128) * w[j]
        coef[d, 7] = bcol

    new_keys(0)
    new_keys(1)
    send_sums(2)
    new_keys(3)
    new_keys(2)

    first_in, peer_in = {}, {}
    for d in (0, 1, 3, 2):
        h = turn(a, -d)
        if d:
            c_in[1, d].wait_recv()
            c_in[2, d].wait_recv()
        v = silu(proj[1, h].astype(F32) * inv_col)
        fresh = mixed(both(coef[d, 7]) * v - zk[d], [both(coef[d, j]) for j in range(3)])
        res = zq[d]
        for j in range(4):
            res = res + both(coef[d, 3 + j]) * back(fresh, j)
        norm = res * lax.rsqrt(jnp.mean(res * res, -1, keepdims=True) + norm_eps) * head_gain[...]
        gath[kv, h] = (norm * silu(proj[2, h].astype(F32) * inv_col)).astype(BF16)
        block = gath.at[kv, h]
        for e in (2, 1, 3):
            first_in[e, d] = sems.go(block, block, (kv_at(turn(a, e), b), tp))
        for e in (2, 1, 3):
            peer_in[e, d] = sems.go(block, block, (kv_at(a, turn(b, e)), tp))

    on_in = {}
    for d in (0, 1, 3, 2):
        for e in (1, 3, 2):
            first_in[e, d].wait_recv()
            src = turn(a, -e)
            block = gath.at[kv_at(src, b), turn(src, -d)]
            for f in (2, 1, 3):
                on_in[e, f, d] = sems.go(block, block, (kv_at(a, turn(b, f)), tp))

    local[2].wait()
    weights = wo[...]
    outs = []

    def send_out(src, waits):
        n = len(outs)
        for copy in waits:
            copy.wait_recv()
        to, half = src // 2, lax.rem(src, 2)
        e = lax.rem(to - tp + 8, 8)
        rows = pl.ds(pl.multiple_of(half * OWN, OWN), OWN)
        total = dot(jnp.concatenate([gath[src, h] for h in range(HD)], 1), weights).astype(BF16)
        osend[n] = total
        copy = pltpu.make_async_remote_copy(
            src_ref=osend.at[n],
            dst_ref=orecv.at[e, rows, :],
            send_sem=o_send.at[n],
            recv_sem=o_recv.at[2 * e + half],
            device_id=(kv, to),
            device_id_type=MESH,
        )
        outs.append((e, copy))

        @pl.when(e != 0)
        def _():
            copy.start()

        @pl.when(e == 0)
        def _():
            orecv[0, rows, :] = total

    send_out(kv, [])
    for e in (1, 3, 2):
        send_out(kv_at(turn(a, -e), b), [])
    for e in (1, 3, 2):
        send_out(kv_at(a, turn(b, -e)), [peer_in[e, d] for d in range(4)])
    for e in (1, 3, 2):
        for f in (1, 3, 2):
            send_out(kv_at(turn(a, -e), turn(b, -f)), [on_in[e, f, d] for d in range(4)])

    for e in range(1, 8):
        for half in (0, 1):
            rows = pl.ds(half * OWN, OWN)
            pltpu.make_async_remote_copy(
                src_ref=osend.at[0],
                dst_ref=orecv.at[e, rows, :],
                send_sem=o_send.at[0],
                recv_sem=o_recv.at[2 * e + half],
                device_id=(kv, lax.rem(tp + e, 8)),
                device_id_type=MESH,
            ).wait_recv()
    total = orecv[0].astype(F32)
    for i in range(1, 8):
        total = total + orecv[i].astype(F32)
    out_ref[...] = total.astype(BF16)
    for copy in sems.sent:
        copy.wait_send()
    for e, copy in outs:

        @pl.when(e != 0)
        def _():
            copy.wait_send()

    assert sems.at == N_SEM, sems.at


def mix(*args):
    hbm = pl.BlockSpec(memory_space=pl.ANY)
    vmem = pl.BlockSpec(memory_space=pltpu.VMEM)
    smem = pl.BlockSpec(memory_space=pltpu.SMEM)
    return pl.pallas_call(
        kernel,
        in_specs=[hbm, vmem] + [hbm] * 7 + [smem, vmem, hbm] + [vmem] * 5,
        out_specs=(vmem, vmem),
        out_shape=(jax.ShapeDtypeStruct((128, 256), BF16), pltpu.VMEM((SEQ, HD, DK, DV), F32)),
        scratch_shapes=[
            pltpu.VMEM((4, TOK, KB), BF16),
            pltpu.VMEM((TOK, 4 * KB), BF16),
            pltpu.VMEM((3, 4 * KB, 256), BF16),
            pltpu.VMEM((4, 2, 4, KB), BF16),
            pltpu.VMEM((SEQ, HD, DK, DV), BF16),
            pltpu.VMEM((HD * DV, 256), BF16),
            pltpu.VMEM((HD, OWN, 128), F32),
            pltpu.VMEM((HD, OWN, 128), F32),
            pltpu.VMEM((HD, OWN, DV), F32),
            pltpu.VMEM((HD, 3, OWN, 128), F32),
            pltpu.VMEM((HD, OWN, 128), F32),
            pltpu.VMEM((3, 4, 256, 256), BF16),
            pltpu.VMEM((3, 3, 256, 256), BF16),
            pltpu.VMEM((4, 16, 128), F32),
            pltpu.VMEM((3, 16, 128), F32),
            pltpu.VMEM((3, 3, OWN, 256), BF16),
            pltpu.VMEM((3, HD, OWN, 256), BF16),
            pltpu.VMEM((4, 8, OWN, 128), F32),
            pltpu.VMEM((4, OWN, DV), F32),
            pltpu.VMEM((4, OWN, DV), F32),
            pltpu.VMEM((16, HD, OWN, DV), BF16),
            pltpu.VMEM((16, OWN, 256), BF16),
            pltpu.VMEM((8, 128, 256), BF16),
            pltpu.SemaphoreType.DMA((N_SEM,)),
            pltpu.SemaphoreType.DMA((N_SEM,)),
            pltpu.SemaphoreType.DMA((9,)),
            pltpu.SemaphoreType.DMA((16,)),
            pltpu.SemaphoreType.DMA((16,)),
        ],
        compiler_params=pltpu.CompilerParams(
            collective_id=0, has_side_effects=True, vmem_limit_bytes=50 * 1024 * 1024
        ),
        name="mix",
    )(*[pltpu.with_memory_space_constraint(arg, pltpu.HBM) for arg in args])


def per_device(
    hidden,
    norm_gain,
    w_query,
    w_key,
    w_value,
    w_gate,
    w_write,
    w_decay,
    w_out,
    decay_rate,
    head_gain,
    carried_state,
    last_keys,
    last_values,
    last_writes,
    last_decays,
    accepted,
):
    mixed_out, committed = mix(
        hidden,
        norm_gain.astype(F32).reshape(16, 1, 256),
        w_query,
        w_key,
        w_value,
        w_gate,
        w_write.T,
        w_decay.T,
        w_out,
        decay_rate,
        head_gain.reshape(1, DV),
        carried_state,
        last_keys,
        last_values,
        jnp.transpose(last_writes, (1, 2, 0)),
        jnp.transpose(last_decays, (1, 2, 0)),
        accepted.reshape(1, SEQ),
    )
    return (mixed_out, committed)


def solution(mesh):
    return jax.shard_map(
        per_device,
        mesh=mesh,
        in_specs=(
            P(None, "kv"),
            P(),
            P("kv", "tp"),
            P("kv", "tp"),
            P("kv", "tp"),
            P("kv", "tp"),
            P("kv", "tp"),
            P("kv", "tp"),
            P("tp", "kv"),
            P("tp"),
            P(),
            P("kv", "tp", None, None),
            P("kv", None, "tp"),
            P("kv", None, "tp"),
            P("kv", None, "tp"),
            P("kv", None, "tp"),
            P("kv"),
        ),
        out_specs=(P("tp", "kv"), P("kv", "tp", None, None)),
        check_vma=False,
    )
```

time: 90.2 us -> 67.9 us (0.75)
  the two profiles are of different devices: /device:TPU:1 before, /device:TPU:17 now
where the time goes in v2:
time: 67.9 us; the launch traced here: 67.7 us
  Pallas kernels  61.7 us (91%)
  local copies, waits for them, and re-layouts  4.03 us (6%)
  other arithmetic  1.3 us (2%)
    pallas_call x1, Pallas kernels, mix(): pl.pallas_call(kernel, in_specs=[hbm, vmem] + [hbm] * 7 + [smem, vmem, hb...  61.7 us
    unnamed x4, local copies, waits for them, and re-layouts  4.03 us

profile of v2, /device:TPU:17, one launch (start us, length us, event | category | flops | bytes accessed | tf_op | source)
XLA Modules:
  0.0 67.7 jit_solution(14682518618171131635)
XLA Ops:
  0.6 1.3 %reshape.19 = f32[4096]{0:T(1024)} convert(bf16[4096]{0:T(1024)(128)(2,1)} %param.18) | non-fusion elementwise | flops 4096 | bytes 24576 | tf_op jit(solution)/shard_map/reshape | solution.py:619
  1.9 61.7 %mix.1 = (bf16[128,256]{1,0:T(8,128)(2,1)}, f32[16,4,128,256]{3,2,1,0:T(8,128)S(1)}) custom-call(bf16[1024,256]{1,0:T(8,128)(2,1)} %hidden.1, f32[16,1,256]{2,1,0:T(1,128)} %bitcast.7, bf16[256,512]{1,0:T(8,128)(2,1)} %w_query.1, bf16[256,512]{1,0:T(8,128)(2,1)} %w_key.1, bf16[256,1024]{1,0:T(8,128)(2,1)} %w_value.1, bf16[256,1024]{1,0:T(8,128)(2,1)} %w_gate.1, ...), custom_call_target="tpu_custom_call" | custom-call | tf_op jit(solution)/shard_map/mix/pallas_call | solution.py:556
  63.7 0.0 copy-start
  63.7 3.4 %copy.21 = f32[16,4,128,256]{3,2,1,0:T(8,128)} copy(f32[16,4,128,256]{3,2,1,0:T(8,128)S(1)} %get-tuple-element.3) | data formatting | bytes 16777216
  67.1 0.0 copy-done
  67.1 0.6 copy.22
Async XLA Ops:
  63.7 3.4 %copy-start = (bf16[128,256]{1,0:T(8,128)(2,1)S(1)}, bf16[128,256]{1,0:T(8,128)(2,1)}, u32[]{:S(2)}) copy-start(bf16[128,256]{1,0:T(8,128)(2,1)} %get-tuple-element.6) | copy-start | bytes 196612

commit v3 on v2

--- a/solution.py
+++ b/solution.py
@@ -154,7 +154,7 @@
     w_write,
     w_decay,
     w_out,
-    rate_ref,
+    decay_rate,
     head_gain,
     state,
     last_keys,
@@ -162,8 +162,17 @@
     last_writes,
     last_decays,
     accepted,
-    out_ref,
+    orecv,
     st32,
+    gain_raw,
+    gain32,
+    rate_row,
+    head_gain_row,
+    old_keys,
+    old_values,
+    old_writes,
+    old_decays,
+    old_count,
     hid,
     scaled,
     wbuf,
@@ -186,7 +195,6 @@
     zq,
     gath,
     osend,
-    orecv,
     send,
     recv,
     loc,
@@ -222,7 +230,19 @@
             (w_gate.at[:, head_cols(h, DV)], wbuf.at[2, own_rows, :]),
         ]
 
-    pairs = [(hidden, hid.at[a]), (state, st32), (w_out, wo)] + weight_parts(a)
+    pairs = [
+        (last_keys, old_keys),
+        (last_values, old_values),
+        (last_writes, old_writes),
+        (last_decays, old_decays),
+        (accepted, old_count),
+        (decay_rate, rate_row),
+        (gain, gain_raw),
+        (head_gain, head_gain_row),
+        (hidden, hid.at[a]),
+        (state, st32),
+        (w_out, wo),
+    ] + weight_parts(a)
     local = [pltpu.make_async_copy(src, dst, loc.at[n]) for n, (src, dst) in enumerate(pairs)]
     for copy in local:
         copy.start()
@@ -250,6 +270,9 @@
             for src, dst in weight_parts(to)[first:past]:
                 w_in[d].append(sems.go(src, dst, (kv_at(to, b), tp)))
 
+    for copy in local[:8]:
+        copy.wait()
+    gain32[...] = gain_raw[...].astype(F32)
     at = place((OWN, 128))
     which = lax.broadcasted_iota(jnp.int32, (OWN, SEQ), 0)
     seq = lax.broadcasted_iota(jnp.int32, (OWN, SEQ), 1)
@@ -257,23 +280,25 @@
     for p in range(4):
         raw = raw + lax.dot_general(
             (which == 4 * seq + p).astype(F32),
-            jnp.concatenate([last_writes[p], last_decays[p]], 0),
+            jnp.concatenate([old_writes[p], old_decays[p]], 0),
             NT,
             precision=HIGHEST,
             preferred_element_type=F32,
         )
-    count = jnp.sum(jnp.where(which // 4 == seq, accepted[...].astype(F32), 0.0), -1, keepdims=True)
+    count = jnp.sum(jnp.where(which // 4 == seq, old_count[...].astype(F32), 0.0), -1, keepdims=True)
     taken = (place((OWN, 8)).astype(F32) < count).astype(F32)
     lane8 = lax.broadcasted_iota(jnp.int32, (OWN, 8), 1)
-    rate = jnp.zeros((OWN, 8), F32)
-    for h in range(HD):
-        rate = jnp.where(lane8 == 4 + h, rate_ref[h], rate)
-    cols = jnp.where(lane8 < 4, sigmoid(raw), -rate * softplus(raw)) * taken
+    rate = jnp.concatenate([rate_row[...], rate_row[...]], 1)
+
+    def rates_and_decays(pre):
+        return jnp.where(lane8 < 4, sigmoid(pre), -rate * softplus(pre))
+
+    cols = rates_and_decays(raw) * taken
 
     for n in range(SEQ // 2):
         rows = slice(8 * n, 8 * n + 8)
-        lhs_pair = [last_keys[2 * n + i].astype(F32) for i in (0, 1)]
-        val_pair = [last_values[2 * n + i].astype(F32) for i in (0, 1)]
+        lhs_pair = [old_keys[2 * n + i].astype(F32) for i in (0, 1)]
+        val_pair = [old_values[2 * n + i].astype(F32) for i in (0, 1)]
         for h in range(HD):
             cut = slice(h * DK, (h + 1) * DK)
             lhs[h, rows, :] = jnp.concatenate([v[:, cut] for v in lhs_pair], 0)
@@ -304,7 +329,7 @@
             sems.go(hid.at[slot, rows, :], hid.at[slot, rows, :], (kv, 2 * turn(y, e) + core)) for e in (1, 3)
         ]
 
-    local[1].wait()
+    local[9].wait()
     row8 = lax.broadcasted_iota(jnp.int32, (8, DV), 0)
     row8k = lax.broadcasted_iota(jnp.int32, (8, DK), 0)
 
@@ -330,7 +355,8 @@
     lax.fori_loop(0, SEQ // 2, old_pair, 0)
 
     def scale_block(slot):
-        weight = gain[kv_at(slot, b)]
+        row = 2 * kv_at(slot, b)
+        weight = jnp.concatenate([gain32[pl.ds(row, 1), :], gain32[pl.ds(row + 1, 1), :]], 1)
 
         def body(n, _):
             kb, ka = n // 4, lax.rem(n, 4)
@@ -342,7 +368,7 @@
 
         lax.fori_loop(0, 16, body, 0)
 
-    local[0].wait()
+    local[8].wait()
     scale_block(a)
     for d in (1, 3, 2):
         hid_in[d, 2].wait_recv()
@@ -353,7 +379,7 @@
     p_in, c_in = {}, {}
 
     def send_parts(chunk, first, past):
-        for copy in local[3 + first : 3 + past]:
+        for copy in local[11 + first : 11 + past]:
             copy.wait()
         for d in (1, 3, 2):
             for copy in w_in[d][first:past]:
@@ -414,15 +440,9 @@
     small = ssend[0]
     for i in range(3):
         small = small + srecv[i]
-    inv = lax.rsqrt(small[8:16] / D + norm_eps)
-    row = lax.broadcasted_iota(jnp.int32, (8, 128), 0)
-    rate = jnp.zeros((8, 128), F32)
-    for h in range(HD):
-        rate = jnp.where(row == 4 + h, rate_ref[h], rate)
-    pre = small[0:8] * inv
-    top = jnp.where(row < 4, sigmoid(pre), -rate * softplus(pre))
-    cols = columns_of(jnp.concatenate([top, inv], 0))
-    inv_col = cols[:, 8:9]
+    small_cols = columns_of(small)
+    inv_col = lax.rsqrt(small_cols[:, 8:9] / D + norm_eps)
+    cols = rates_and_decays(small_cols[:, 0:8] * inv_col)
     send_sums(1)
 
     def new_keys(d):
@@ -466,7 +486,7 @@
         res = zq[d]
         for j in range(4):
             res = res + both(coef[d, 3 + j]) * back(fresh, j)
-        norm = res * lax.rsqrt(jnp.mean(res * res, -1, keepdims=True) + norm_eps) * head_gain[...]
+        norm = res * lax.rsqrt(jnp.mean(res * res, -1, keepdims=True) + norm_eps) * head_gain_row[...]
         gath[kv, h] = (norm * silu(proj[2, h].astype(F32) * inv_col)).astype(BF16)
         block = gath.at[kv, h]
         for e in (2, 1, 3):
@@ -483,7 +503,7 @@
             for f in (2, 1, 3):
                 on_in[e, f, d] = sems.go(block, block, (kv_at(a, turn(b, f)), tp))
 
-    local[2].wait()
+    local[10].wait()
     weights = wo[...]
     outs = []
 
@@ -534,10 +554,6 @@
                 device_id=(kv, lax.rem(tp + e, 8)),
                 device_id_type=MESH,
             ).wait_recv()
-    total = orecv[0].astype(F32)
-    for i in range(1, 8):
-        total = total + orecv[i].astype(F32)
-    out_ref[...] = total.astype(BF16)
     for copy in sems.sent:
         copy.wait_send()
     for e, copy in outs:
@@ -552,13 +568,21 @@
 def mix(*args):
     hbm = pl.BlockSpec(memory_space=pl.ANY)
     vmem = pl.BlockSpec(memory_space=pltpu.VMEM)
-    smem = pl.BlockSpec(memory_space=pltpu.SMEM)
     return pl.pallas_call(
         kernel,
-        in_specs=[hbm, vmem] + [hbm] * 7 + [smem, vmem, hbm] + [vmem] * 5,
+        in_specs=[hbm] * 17,
         out_specs=(vmem, vmem),
-        out_shape=(jax.ShapeDtypeStruct((128, 256), BF16), pltpu.VMEM((SEQ, HD, DK, DV), F32)),
+        out_shape=(pltpu.VMEM((8, 128, 256), BF16), pltpu.VMEM((SEQ, HD, DK, DV), F32)),
         scratch_shapes=[
+            pltpu.VMEM((32, 128), BF16),
+            pltpu.VMEM((32, 128), F32),
+            pltpu.VMEM((1, HD), F32),
+            pltpu.VMEM((1, DV), F32),
+            pltpu.VMEM((SEQ, 4, HD * DK), BF16),
+            pltpu.VMEM((SEQ, 4, HD * DV), BF16),
+            pltpu.VMEM((4, HD, SEQ), F32),
+            pltpu.VMEM((4, HD, SEQ), F32),
+            pltpu.VMEM((1, SEQ), jnp.int32),
             pltpu.VMEM((4, TOK, KB), BF16),
             pltpu.VMEM((TOK, 4 * KB), BF16),
             pltpu.VMEM((3, 4 * KB, 256), BF16),
@@ -581,10 +605,9 @@
             pltpu.VMEM((4, OWN, DV), F32),
             pltpu.VMEM((16, HD, OWN, DV), BF16),
             pltpu.VMEM((16, OWN, 256), BF16),
-            pltpu.VMEM((8, 128, 256), BF16),
             pltpu.SemaphoreType.DMA((N_SEM,)),
             pltpu.SemaphoreType.DMA((N_SEM,)),
-            pltpu.SemaphoreType.DMA((9,)),
+            pltpu.SemaphoreType.DMA((17,)),
             pltpu.SemaphoreType.DMA((16,)),
             pltpu.SemaphoreType.DMA((16,)),
         ],
@@ -593,6 +616,35 @@
         ),
         name="mix",
     )(*[pltpu.with_memory_space_constraint(arg, pltpu.HBM) for arg in args])
+
+
+def write_kernel(parts, states, out_ref, committed, rows, sem):
+    copies = [pltpu.make_async_copy(states.at[n], committed.at[n], sem.at[n]) for n in range(SEQ)]
+    for copy in copies:
+        copy.start()
+    total = parts[0].astype(F32)
+    for i in range(1, 8):
+        total = total + parts[i].astype(F32)
+    rows[...] = total.astype(BF16)
+    copy = pltpu.make_async_copy(rows, out_ref, sem.at[SEQ])
+    copy.start()
+    for other in copies:
+        other.wait()
+    copy.wait()
+
+
+def write_out(parts, states):
+    hbm = pl.BlockSpec(memory_space=pltpu.HBM)
+    vmem = pl.BlockSpec(memory_space=pltpu.VMEM)
+    return pl.pallas_call(
+        write_kernel,
+        in_specs=[vmem, vmem],
+        out_specs=(hbm, hbm),
+        out_shape=(jax.ShapeDtypeStruct((128, 256), BF16), jax.ShapeDtypeStruct((SEQ, HD, DK, DV), F32)),
+        scratch_shapes=[pltpu.VMEM((128, 256), BF16), pltpu.SemaphoreType.DMA((SEQ + 1,))],
+        compiler_params=pltpu.CompilerParams(vmem_limit_bytes=4 * 1024 * 1024),
+        name="write_out",
+    )(*[pltpu.with_memory_space_constraint(arg, pltpu.VMEM) for arg in (parts, states)])
 
 
 def per_device(
@@ -614,9 +666,9 @@
     last_decays,
     accepted,
 ):
-    mixed_out, committed = mix(
+    parts, states = mix(
         hidden,
-        norm_gain.astype(F32).reshape(16, 1, 256),
+        norm_gain.reshape(32, 128),
         w_query,
         w_key,
         w_value,
@@ -624,7 +676,7 @@
         w_write.T,
         w_decay.T,
         w_out,
-        decay_rate,
+        decay_rate.reshape(1, HD),
         head_gain.reshape(1, DV),
         carried_state,
         last_keys,
@@ -633,7 +685,7 @@
         jnp.transpose(last_decays, (1, 2, 0)),
         accepted.reshape(1, SEQ),
     )
-    return (mixed_out, committed)
+    return write_out(parts, states)
 
 
 def solution(mesh):

time: 67.9 us -> 64.4 us (0.948)
  local copies, waits for them, and re-layouts: 4.03 us -> 0 us
  Pallas kernels: 61.7 us -> 63.7 us
  other arithmetic: 1.3 us -> 0 us
    unnamed x4 -> x0, local copies, waits for them, and re-layouts: 4.03 us -> none
    pallas_call x1 -> x2, Pallas kernels: 61.7 us -> 63.7 us  [the longest x1 60.3 us: mix(): pl.pallas_call(kernel, in_specs=[hbm] * 17, out_specs=(vmem, vmem), out_s...]
    reshape x1 -> x0, other arithmetic: 1.3 us -> none  [per_device(): norm_gain.astype(F32).reshape(16, 1, 256)]
where the time goes in v3:
time: 64.4 us; the launch traced here: 64.3 us
  Pallas kernels  63.7 us (99%)
  between operations  0.65 us (1%)
    pallas_call x1, Pallas kernels, mix(): pl.pallas_call(kernel, in_specs=[hbm] * 17, out_specs=(vmem, vmem), out_s...  60.3 us
    pallas_call x1, Pallas kernels, write_out(): pl.pallas_call(write_kernel, in_specs=[vmem, vmem], out_specs=(hbm, hbm),...  3.43 us

profile of v3, /device:TPU:17, one launch (start us, length us, event | category | flops | bytes accessed | tf_op | source)
XLA Modules:
  0.0 64.3 jit_solution(5416014846873796344)
XLA Ops:
  0.6 60.3 %mix.1 = (bf16[8,128,256]{2,1,0:T(8,128)(2,1)S(1)}, f32[16,4,128,256]{3,2,1,0:T(8,128)S(1)}) custom-call(bf16[1024,256]{1,0:T(8,128)(2,1)} %hidden.1, bf16[32,128]{1,0:T(8,128)(2,1)} %bitcast.8, bf16[256,512]{1,0:T(8,128)(2,1)} %w_query.1, bf16[256,512]{1,0:T(8,128)(2,1)} %w_key.1, bf16[256,1024]{1,0:T(8,128)(2,1)} %w_value.1, bf16[256,1024]{1,0:T(8,128)(2,1)} %w_gate.1, ...), custom_call_target="tpu_custom_call" | custom-call | tf_op jit(solution)/shard_map/mix/pallas_call | solution.py:571
  60.9 3.4 %write_out.1 = (bf16[128,256]{1,0:T(8,128)(2,1)}, f32[16,4,128,256]{3,2,1,0:T(8,128)}) custom-call(bf16[8,128,256]{2,1,0:T(8,128)(2,1)S(1)} %get-tuple-element.4.parts, f32[16,4,128,256]{3,2,1,0:T(8,128)S(1)} %get-tuple-element.5.states), custom_call_target="tpu_custom_call" | custom-call | tf_op jit(solution)/shard_map/write_out/pallas_call | solution.py:639

commit v4 on v3

--- a/solution.py
+++ b/solution.py
@@ -140,7 +140,7 @@
         return copy
 
 
-N_SEM = 6 + 3 * 6 + 6 + 9 + 3 + 9 + 12 + 12 + 36
+N_SEM = 6 + 3 * 6 + 6 + 9 + 3 + 9 + 2 * 19 + 30
 NT = (((1,), (1,)), ((), ()))
 
 
@@ -475,8 +475,23 @@
     new_keys(3)
     new_keys(2)
 
-    first_in, peer_in = {}, {}
-    for d in (0, 1, 3, 2):
+    def gated(ea, fb, d):
+        src = turn(a, -ea)
+        return gath.at[kv_at(src, turn(b, -fb)), turn(src, -d)]
+
+    def along_a(s):
+        return (kv_at(turn(a, s), b), tp)
+
+    def along_b(s):
+        return (kv_at(a, turn(b, s)), tp)
+
+    def half_of(block, s):
+        return block.at[pl.ds(OWN // 2 * (s // 2), OWN // 2), :]
+
+    b_near, b_far = {}, {}
+    first_in, peer_in, on_in = {}, {}, {}
+
+    def new_rows(d):
         h = turn(a, -d)
         if d:
             c_in[1, d].wait_recv()
@@ -488,20 +503,61 @@
             res = res + both(coef[d, 3 + j]) * back(fresh, j)
         norm = res * lax.rsqrt(jnp.mean(res * res, -1, keepdims=True) + norm_eps) * head_gain_row[...]
         gath[kv, h] = (norm * silu(proj[2, h].astype(F32) * inv_col)).astype(BF16)
-        block = gath.at[kv, h]
+
+    def b_first(ea, d):
+        block = gated(ea, 0, d)
+        for s in (1, 3):
+            b_near[ea, s, d] = sems.go(block, block, along_b(s))
+
+    def b_relay(ea, d):
+        for s in (1, 3):
+            b_near[ea, s, d].wait_recv()
+            block = half_of(gated(ea, s, d), s)
+            b_far[ea, s, d] = sems.go(block, block, along_b(s))
+
+    def start(d, direct=False):
+        new_rows(d)
+        block = gated(0, 0, d)
         for e in (2, 1, 3):
-            first_in[e, d] = sems.go(block, block, (kv_at(turn(a, e), b), tp))
-        for e in (2, 1, 3):
-            peer_in[e, d] = sems.go(block, block, (kv_at(a, turn(b, e)), tp))
-
-    on_in = {}
-    for d in (0, 1, 3, 2):
+            first_in[e, d] = sems.go(block, block, along_a(e))
+        if direct:
+            for e in (2, 1, 3):
+                peer_in[e, d] = sems.go(block, block, along_b(e))
+        else:
+            b_first(0, d)
+
+    def hand_on(d, direct=False):
         for e in (1, 3, 2):
             first_in[e, d].wait_recv()
-            src = turn(a, -e)
-            block = gath.at[kv_at(src, b), turn(src, -d)]
-            for f in (2, 1, 3):
-                on_in[e, f, d] = sems.go(block, block, (kv_at(a, turn(b, f)), tp))
+            if direct:
+                block = gated(e, 0, d)
+                for f in (2, 1, 3):
+                    on_in[e, f, d] = sems.go(block, block, along_b(f))
+            else:
+                b_first(e, d)
+
+    start(0)
+    start(1)
+    start(3, True)
+    start(2, True)
+    for d in (0, 1):
+        b_relay(0, d)
+        hand_on(d)
+    hand_on(3, True)
+    hand_on(2, True)
+    for d in (0, 1):
+        for e in (1, 3, 2):
+            b_relay(e, d)
+
+    def arrived(ea, fb):
+        waits = []
+        if fb == 2:
+            waits += [b_far[ea, s, d] for d in (0, 1) for s in (1, 3)]
+        if fb and ea:
+            waits += [on_in[ea, fb, 3], on_in[ea, fb, 2]]
+        elif fb:
+            waits += [peer_in[fb, 3], peer_in[fb, 2]]
+        return waits
 
     local[10].wait()
     weights = wo[...]
@@ -534,14 +590,11 @@
         def _():
             orecv[0, rows, :] = total
 
-    send_out(kv, [])
-    for e in (1, 3, 2):
-        send_out(kv_at(turn(a, -e), b), [])
-    for e in (1, 3, 2):
-        send_out(kv_at(a, turn(b, -e)), [peer_in[e, d] for d in range(4)])
-    for e in (1, 3, 2):
-        for f in (1, 3, 2):
-            send_out(kv_at(turn(a, -e), turn(b, -f)), [on_in[e, f, d] for d in range(4)])
+    for ea, fb in ((0, 0), (1, 0), (3, 0), (2, 0), (0, 1), (0, 3), (0, 2)):
+        send_out(kv_at(turn(a, -ea), turn(b, -fb)), arrived(ea, fb))
+    for fb in (1, 3, 2):
+        for ea in (1, 3, 2):
+            send_out(kv_at(turn(a, -ea), turn(b, -fb)), arrived(ea, fb))
 
     for e in range(1, 8):
         for half in (0, 1):

time: 64.4 us -> 63.3 us (0.983)
  Pallas kernels: 63.7 us -> 62.4 us
    pallas_call x1, Pallas kernels: 60.3 us -> 58.9 us  [mix(): pl.pallas_call(kernel, in_specs=[hbm] * 17, out_specs=(vmem, vmem), out_s...]
where the time goes in v4:
time: 63.3 us; the launch traced here: 63 us
  Pallas kernels  62.4 us (99%)
  between operations  0.65 us (1%)
    pallas_call x1, Pallas kernels, mix(): pl.pallas_call(kernel, in_specs=[hbm] * 17, out_specs=(vmem, vmem), out_s...  58.9 us
    pallas_call x1, Pallas kernels, write_out(): pl.pallas_call(write_kernel, in_specs=[vmem, vmem], out_specs=(hbm, hbm),...  3.43 us

profile of v4, /device:TPU:17, one launch (start us, length us, event | category | flops | bytes accessed | tf_op | source)
XLA Modules:
  0.0 63.0 jit_solution(4286748451854660796)
XLA Ops:
  0.6 58.9 %mix.1 = (bf16[8,128,256]{2,1,0:T(8,128)(2,1)S(1)}, f32[16,4,128,256]{3,2,1,0:T(8,128)S(1)}) custom-call(bf16[1024,256]{1,0:T(8,128)(2,1)} %hidden.1, bf16[32,128]{1,0:T(8,128)(2,1)} %bitcast.8, bf16[256,512]{1,0:T(8,128)(2,1)} %w_query.1, bf16[256,512]{1,0:T(8,128)(2,1)} %w_key.1, bf16[256,1024]{1,0:T(8,128)(2,1)} %w_value.1, bf16[256,1024]{1,0:T(8,128)(2,1)} %w_gate.1, ...), custom_call_target="tpu_custom_call" | custom-call | tf_op jit(solution)/shard_map/mix/pallas_call | solution.py:624
  59.6 3.4 %write_out.1 = (bf16[128,256]{1,0:T(8,128)(2,1)}, f32[16,4,128,256]{3,2,1,0:T(8,128)}) custom-call(bf16[8,128,256]{2,1,0:T(8,128)(2,1)S(1)} %get-tuple-element.4.parts, f32[16,4,128,256]{3,2,1,0:T(8,128)S(1)} %get-tuple-element.5.states), custom_call_target="tpu_custom_call" | custom-call | tf_op jit(solution)/shard_map/write_out/pallas_call | solution.py:692

commit v5 on v4

--- a/solution.py
+++ b/solution.py
@@ -140,7 +140,7 @@
         return copy
 
 
-N_SEM = 6 + 3 * 6 + 6 + 9 + 3 + 9 + 2 * 19 + 30
+N_SEM = 12 + 3 * 6 + 12 + 9 + 3 + 9 + 2 * 19 + 30
 NT = (((1,), (1,)), ((), ()))
 
 
@@ -259,10 +259,17 @@
         return pl.ds(pl.multiple_of(i * 256, 256), 256)
 
     hid_in = {}
+
+    def rows_of(i, part):
+        return pl.ds(pl.multiple_of(i * 256 + part * 128, 128), 128)
+
     for e in (0, 2):
-        for d in (1, 3, 2):
-            rows = quarter(turn(y, e))
-            hid_in[d, e] = sems.go(hidden.at[rows, :], hid.at[a, rows, :], (kv_at(turn(a, d), b), tp))
+        for part in (0, 1):
+            for d in (1, 3, 2):
+                rows = rows_of(turn(y, e), part)
+                hid_in[d, e, part] = sems.go(
+                    hidden.at[rows, :], hid.at[a, rows, :], (kv_at(turn(a, d), b), tp)
+                )
     w_in = {d: [] for d in (1, 2, 3)}
     for first, past in ((0, 4), (4, 5), (5, 6)):
         for d in (2, 1, 3):
@@ -305,6 +312,14 @@
             cut = slice(h * DV, (h + 1) * DV)
             bv[h, rows, :] = jnp.concatenate([v[:, cut] for v in val_pair], 0)
 
+    y_in = {1: [], 2: [], 3: []}
+    for part in (0, 1):
+        for d in (1, 3, 2):
+            hid_in[d, 0, part].wait_recv()
+            block = hid.at[turn(a, -d), rows_of(y, part), :]
+            for e in (1, 3):
+                y_in[d].append(sems.go(block, block, (kv, 2 * turn(y, e) + core)))
+
     def old_head(h, _):
         bcol, g = pick(cols, h), pick(cols, h + 4)
         k = unit(lhs[h])
@@ -319,15 +334,6 @@
         return 0
 
     lax.fori_loop(0, HD, old_head, 0)
-
-    y_in = {}
-    for d in (1, 3, 2):
-        hid_in[d, 0].wait_recv()
-        slot = turn(a, -d)
-        rows = quarter(y)
-        y_in[d] = [
-            sems.go(hid.at[slot, rows, :], hid.at[slot, rows, :], (kv, 2 * turn(y, e) + core)) for e in (1, 3)
-        ]
 
     local[9].wait()
     row8 = lax.broadcasted_iota(jnp.int32, (8, DV), 0)
@@ -371,7 +377,8 @@
     local[8].wait()
     scale_block(a)
     for d in (1, 3, 2):
-        hid_in[d, 2].wait_recv()
+        hid_in[d, 2, 0].wait_recv()
+        hid_in[d, 2, 1].wait_recv()
         for copy in y_in[d]:
             copy.wait_recv()
         scale_block(turn(a, -d))

time: 63.3 us -> 63.4 us (level)
  no operation moved by 1% of the time
where the time goes in v5:
time: 63.4 us; the launch traced here: 63.3 us
  Pallas kernels  62.6 us (99%)
  between operations  0.65 us (1%)
    pallas_call x1, Pallas kernels, mix(): pl.pallas_call(kernel, in_specs=[hbm] * 17, out_specs=(vmem, vmem), out_s...  59.2 us
    pallas_call x1, Pallas kernels, write_out(): pl.pallas_call(write_kernel, in_specs=[vmem, vmem], out_specs=(hbm, hbm),...  3.43 us

profile of v5, /device:TPU:17, one launch (start us, length us, event | category | flops | bytes accessed | tf_op | source)
XLA Modules:
  0.0 63.3 jit_solution(14494036282588762031)
XLA Ops:
  0.6 59.2 %mix.1 = (bf16[8,128,256]{2,1,0:T(8,128)(2,1)S(1)}, f32[16,4,128,256]{3,2,1,0:T(8,128)S(1)}) custom-call(bf16[1024,256]{1,0:T(8,128)(2,1)} %hidden.1, bf16[32,128]{1,0:T(8,128)(2,1)} %bitcast.8, bf16[256,512]{1,0:T(8,128)(2,1)} %w_query.1, bf16[256,512]{1,0:T(8,128)(2,1)} %w_key.1, bf16[256,1024]{1,0:T(8,128)(2,1)} %w_value.1, bf16[256,1024]{1,0:T(8,128)(2,1)} %w_gate.1, ...), custom_call_target="tpu_custom_call" | custom-call | tf_op jit(solution)/shard_map/mix/pallas_call | solution.py:631
  59.8 3.4 %write_out.1 = (bf16[128,256]{1,0:T(8,128)(2,1)}, f32[16,4,128,256]{3,2,1,0:T(8,128)}) custom-call(bf16[8,128,256]{2,1,0:T(8,128)(2,1)S(1)} %get-tuple-element.4.parts, f32[16,4,128,256]{3,2,1,0:T(8,128)S(1)} %get-tuple-element.5.states), custom_call_target="tpu_custom_call" | custom-call | tf_op jit(solution)/shard_map/write_out/pallas_call | solution.py:699
